TPU v7x, 512 devices: a whole 4x8x8 slice. The times are simulated.
512 devices in a mesh: ep: 32 (over z, x), tp: 16 (over y, core).
Axes of the slice: x: 4, y: 8, z: 8, core: 2. Of those that a mesh axis runs over, the one named last changes fastest.
Arguments:
- receptance: bfloat16 [8192, 1024], P('ep', 'tp'), may hold values from -6 to 6
- head_key_input: bfloat16 [8192, 1024], P('ep', 'tp'), may hold values from -12 to 12
- head_value_input: bfloat16 [8192, 1024], P('ep', 'tp'), may hold values from -6 to 6
- decay_input_part: bfloat16 [8192, 1024], P('ep', 'tp'), may hold values from -4 to 4
- learning_rate_input: bfloat16 [8192, 1024], P('ep', 'tp'), may hold values from -7 to 1
- output_gate_input: bfloat16 [8192, 1024], P('ep', 'tp'), may hold values from -6 to 6
- decay_channel_offset: float32 [1024], P('tp'), may hold values from -12.5 to -2
- spike_log_decay: float32 [8192, 1024], P('ep', 'tp'), may hold values from -0.7 to 0
- head_norm_gain: float32 [1024], P('tp'), may hold values from 0.1 to 1.9
- head_output_weight: bfloat16 [1024, 2048], P('tp'), may hold values from -0.25 to 0.25
- projection_norm_gain: float32 [2048], replicated, may hold values from 0.1 to 1.9
- expert_input_rows: bfloat16 [4096, 2048], P('ep'), may hold values from -6 to 6
- expert_norm_gain: float32 [2048], replicated, may hold values from 0.1 to 1.9
- selected_expert_index: int32 [4096, 2], P('ep'), may hold values from 0 to 255, all different within a row; in each aligned block of 128 rows (0 to 127, 128 to 255, ...) at most 2 rows name the same one
- selected_expert_weight: float32 [4096, 2], P('ep'), may hold values from 0.3 to 1.5
- routed_gate_weight: bfloat16 [512, 2048, 256], P(('ep', 'tp')), may hold values from -0.125 to 0.125
- routed_up_weight: bfloat16 [512, 2048, 256], P(('ep', 'tp')), may hold values from -0.125 to 0.125
- routed_down_weight: bfloat16 [512, 256, 2048], P(('ep', 'tp')), may hold values from -0.25 to 0.25
- common_gate_weight: bfloat16 [2048, 1024], P(None, 'tp'), may hold values from -0.125 to 0.125
- common_up_weight: bfloat16 [2048, 1024], P(None, 'tp'), may hold values from -0.125 to 0.125
- common_down_weight: bfloat16 [1024, 2048], P('tp'), may hold values from -0.25 to 0.25
Outputs:
- attention_output: bfloat16 [8192, 2048], P(('ep', 'tp'))
- expert_output: bfloat16 [4096, 2048], P('ep', 'tp')
Inputs may be any that keep to these rules, and one draw needn't show every extreme that they name: `selected_expert_index`: each row names 2 different experts. Among the rows of one index of ep (aligned blocks of 128 rows) no expert is named by more than 2 rows, a bound that some block reaches.
All inputs are finite; a program needn't handle non-finite values.
Results may differ from a plain program's by a relative error of at most 0.023.
Values may be sent and summed in bfloat16 or wider, within the bound.
A program may use at most 64 MiB of HBM per device.

v0:
```python
import jax
import jax.numpy as jnp
from jax import lax
from jax.sharding import PartitionSpec as P

HEAD_CHANNELS = 64
BLOCK = 64


NORM_EPSILON = 1e-06
GROUP_EPSILON = 0.00064


def sent_to_all(x, axis):
    copies = jnp.broadcast_to(x, (lax.axis_size(axis), *x.shape))
    return lax.all_to_all(copies, axis, split_axis=0, concat_axis=0, tiled=True)


def collected_together(x, axis):
    leaves = jax.tree.leaves(x)
    order = sorted(range(len(leaves)), key=lambda k: -leaves[k].size)
    width = (1, *leaves[order[0]].shape)[-1]
    lines = [
        jnp.pad(leaves[k].reshape(-1), (0, -leaves[k].size % width)).reshape(-1, width)
        for k in order
    ]
    both, at, found = (sent_to_all(jnp.concatenate(lines), axis), 0, {})
    for k, line in zip(order, lines):
        share = both[:, at : at + len(line)].reshape(len(both), -1)
        found[k] = share[:, : leaves[k].size].reshape(-1, *leaves[k].shape)
        at += len(line)
    numbers = iter(range(len(leaves)))
    return jax.tree.map(lambda _: found[next(numbers)], x)


def folded_in_pairs(pieces, combine):
    while len(jax.tree.leaves(pieces)[0]) > 1:
        pieces = jax.vmap(combine)(
            *(jax.tree.map(lambda part: part[side::2], pieces) for side in (0, 1))
        )
    return jax.tree.map(lambda part: part[0], pieces)


def carried_in(x, axis, combine, identity):
    size, place = (lax.axis_size(axis), lax.axis_index(axis))
    passed = jnp.arange(size) < place

    def kept(part, zero, own):
        part = jnp.where(
            passed.reshape(-1, *(1 for _ in own.shape)),
            part.astype(own.dtype),
            jnp.asarray(zero, own.dtype),
        )
        return part

    pieces = collected_together(
        jax.tree.map(lambda part, kind: part.astype(kind), x, (jnp.bfloat16, jnp.bfloat16)), axis
    )
    return folded_in_pairs(jax.tree.map(kept, pieces, identity, x), combine)


def in_blocks(x, dim, size):
    before, after = (x.shape[:dim], x.shape[dim + 1 :])
    return jnp.moveaxis(x.reshape(*before, size, -1, *after), dim, 0)


def sent_and_summed(x, axis, dim):
    size = lax.axis_size(axis)
    blocks = lax.all_to_all(in_blocks(x, dim, size), axis, 0, 0, tiled=True)
    return jnp.sum(blocks.astype(jnp.float32), axis=0)


def rms_scale(values, gain):
    values = values.astype(jnp.float32)
    return (
        values * lax.rsqrt(jnp.mean(values * values, axis=-1, keepdims=True) + NORM_EPSILON) * gain
    )


def pairwise(first, second, spans):
    return jnp.einsum("htc,hsc,htsc->hts", first, second, spans)


def within_block(state, inputs):
    recept, insertion, value_aug, removal, scaled_removal, decay_logarithm = inputs
    sequence_length = recept.shape[1]
    target = jnp.arange(sequence_length)[:, None]
    source = jnp.arange(sequence_length)[None, :]
    strict = (source < target)[None, :, :, None]
    inclusive = (source <= target)[None, :, :, None]
    cumul = jnp.cumsum(decay_logarithm, axis=1)
    before = cumul - decay_logarithm
    negated = -removal
    span_strict = jnp.exp(jnp.where(strict, before[:, :, None, :] - cumul[:, None, :, :], -jnp.inf))
    span_inclusive = jnp.exp(
        jnp.where(inclusive, cumul[:, :, None, :] - cumul[:, None, :, :], -jnp.inf)
    )
    lower_beta = pairwise(negated, scaled_removal, span_strict)
    lower_key = pairwise(negated, insertion, span_strict)
    output_beta = pairwise(recept, scaled_removal, span_inclusive)
    output_key = pairwise(recept, insertion, span_inclusive)
    right_side = jnp.einsum("htc,hrc->htr", jnp.exp(before) * negated, state)
    right_side = right_side + jnp.einsum("hts,hsr->htr", lower_key, value_aug)
    identity = jnp.eye(sequence_length, dtype=jnp.float32)
    correction = jax.scipy.linalg.solve_triangular(
        identity - lower_beta, right_side, lower=True, unit_diagonal=True
    )
    output = jnp.einsum("htc,hrc->htr", jnp.exp(cumul) * recept, state)
    output = output + jnp.einsum("hts,hsr->htr", output_beta, correction)
    output = output + jnp.einsum("hts,hsr->htr", output_key, value_aug)
    to_end = jnp.exp(cumul[:, -1:, :] - cumul)
    new_state = state * jnp.exp(cumul[:, -1:, :])
    new_state = new_state + jnp.einsum("hsr,hsc->hrc", correction, scaled_removal * to_end)
    new_state = new_state + jnp.einsum("hsr,hsc->hrc", value_aug, insertion * to_end)
    return (new_state, output)


def compose(earlier, later):
    early_map, early_state = earlier
    late_map, late_state = later
    joined_map = jnp.einsum("hij,hjk->hik", early_map, late_map)
    joined_state = jnp.einsum("hvj,hjk->hvk", early_state, late_map) + late_state
    return (joined_map, joined_state)


def attention_mixer(
    receptance,
    head_key_input,
    head_value_input,
    decay_input_part,
    learning_rate_input,
    output_gate_input,
    decay_channel_offset,
    spike_log_decay,
    head_norm_gain,
    head_output_weight,
    projection_norm_gain,
):
    sequence_length, width = receptance.shape
    number_of_heads = width // HEAD_CHANNELS
    block_count = sequence_length // BLOCK

    def reshape_into_blocks(values):
        return (
            values.astype(jnp.float32)
            .reshape(block_count, BLOCK, number_of_heads, HEAD_CHANNELS)
            .transpose(0, 2, 1, 3)
        )

    recept = reshape_into_blocks(receptance)
    keys = reshape_into_blocks(head_key_input)
    values = reshape_into_blocks(head_value_input)
    learn_rate = jax.nn.sigmoid(reshape_into_blocks(learning_rate_input))
    decay_preactivation = decay_channel_offset[None, :] + jnp.tanh(
        decay_input_part.astype(jnp.float32)
    )
    decay_logarithm = reshape_into_blocks(
        spike_log_decay - jnp.exp(-jax.nn.softplus(-decay_preactivation) - 0.5)
    )
    removal = keys * lax.rsqrt(jnp.sum(keys * keys, axis=-1, keepdims=True) + NORM_EPSILON)
    value_aug = jnp.concatenate([values, jnp.zeros_like(values)], axis=-1)
    identity = jnp.broadcast_to(
        jnp.eye(HEAD_CHANNELS, dtype=jnp.float32), (number_of_heads, HEAD_CHANNELS, HEAD_CHANNELS)
    )
    start = jnp.concatenate([jnp.zeros_like(identity), identity], axis=1)
    final, outputs = lax.scan(
        within_block,
        start,
        (recept, keys * learn_rate, value_aug, removal, removal * learn_rate, decay_logarithm),
    )
    _, carried = carried_in(
        (final[:, HEAD_CHANNELS:], final[:, :HEAD_CHANNELS]),
        "ep",
        compose,
        (identity, jnp.zeros_like(identity)),
    )
    head_value = outputs[..., :HEAD_CHANNELS] + jnp.einsum(
        "bhtj,hvj->bhtv", outputs[..., HEAD_CHANNELS:], carried
    )
    centred = head_value - jnp.mean(head_value, axis=-1, keepdims=True)
    normed = centred * lax.rsqrt(
        jnp.mean(centred * centred, axis=-1, keepdims=True) + GROUP_EPSILON
    )
    flat = normed.transpose(0, 2, 1, 3).reshape(sequence_length, width)
    heads_out = (
        flat * head_norm_gain * jax.nn.sigmoid(output_gate_input.astype(jnp.float32))
    ).astype(jnp.bfloat16)
    mix_sum = sent_and_summed(
        jnp.dot(heads_out, head_output_weight, preferred_element_type=jnp.float32).astype(
            jnp.bfloat16
        ),
        "tp",
        0,
    )
    return rms_scale(mix_sum, projection_norm_gain).astype(jnp.bfloat16)


def expert_half(
    expert_input_rows,
    expert_norm_gain,
    selected_expert_index,
    selected_expert_weight,
    routed_gate_weight,
    routed_up_weight,
    routed_down_weight,
    common_gate_weight,
    common_up_weight,
    common_down_weight,
):
    tok_rows, model_width = expert_input_rows.shape
    chosen_count = selected_expert_index.shape[1]
    ep_count = lax.axis_size("ep")
    tp_count = lax.axis_size("tp")
    group_count = tp_count // 2
    expert_total = group_count * ep_count
    capacity = 2 * tok_rows * chosen_count // expert_total
    column_count = model_width // tp_count
    tp_place = lax.axis_index("tp")
    group_index = tp_place // 2
    normed = rms_scale(expert_input_rows, expert_norm_gain).astype(jnp.bfloat16)
    assigned = selected_expert_index.reshape(-1)
    assign_count = assigned.shape[0]
    expert_ids = jnp.arange(expert_total, dtype=jnp.int32)
    onehot = (assigned[:, None] == expert_ids[None, :]).astype(jnp.int32)
    ranking = jnp.sum((jnp.cumsum(onehot, axis=0) - onehot) * onehot, axis=1)
    slot = assigned * capacity + ranking
    owner = (
        jnp.full((expert_total * capacity,), tok_rows, jnp.int32)
        .at[slot]
        .set(jnp.arange(assign_count, dtype=jnp.int32) // chosen_count)
    )
    owner_grid = owner.reshape(ep_count, group_count, capacity)
    mine = lax.dynamic_index_in_dim(owner_grid, group_index, 1, keepdims=False)
    filled = mine < tok_rows
    rows = jnp.take(normed, jnp.minimum(mine, tok_rows - 1), axis=0)
    outgoing = jnp.where(filled[:, :, None], rows, jnp.zeros_like(rows))
    arrived = lax.all_to_all(outgoing, "ep", split_axis=0, concat_axis=0, tiled=True)
    flat_rows = arrived.reshape(-1, model_width)
    gate = jnp.dot(flat_rows, routed_gate_weight[0], preferred_element_type=jnp.float32)
    upward = jnp.dot(flat_rows, routed_up_weight[0], preferred_element_type=jnp.float32)
    hidden = (jax.nn.silu(gate) * upward).astype(jnp.bfloat16)
    partial_value = jnp.dot(
        hidden, routed_down_weight[0], preferred_element_type=jnp.float32
    ).astype(jnp.bfloat16)
    pieces = lax.all_to_all(partial_value[None], "tp", split_axis=2, concat_axis=0, tiled=True)
    paired = pieces.reshape(group_count, 2, ep_count * capacity, column_count).astype(jnp.float32)
    expert_value = (
        (paired[:, 0] + paired[:, 1])
        .astype(jnp.bfloat16)
        .reshape(group_count, ep_count, capacity, column_count)
    )
    returned = lax.all_to_all(expert_value, "ep", split_axis=1, concat_axis=1, tiled=True)
    flat_back = returned.reshape(-1, column_count)
    position = (
        assigned % group_count * (ep_count * capacity)
        + assigned // group_count * capacity
        + ranking
    )
    picked = (
        jnp.take(flat_back, position, axis=0)
        .astype(jnp.float32)
        .reshape(tok_rows, chosen_count, column_count)
    )
    routed = jnp.sum(picked * selected_expert_weight[:, :, None], axis=1)
    shared_hidden = (
        jax.nn.silu(jnp.dot(normed, common_gate_weight, preferred_element_type=jnp.float32))
        * jnp.dot(normed, common_up_weight, preferred_element_type=jnp.float32)
    ).astype(jnp.bfloat16)
    shared_sum = sent_and_summed(
        lax.dot_general(
            common_down_weight,
            shared_hidden,
            (((0,), (1,)), ((), ())),
            preferred_element_type=jnp.float32,
        ).astype(jnp.bfloat16),
        "tp",
        0,
    )
    return (routed + shared_sum.T).astype(jnp.bfloat16)


def body(
    receptance,
    head_key_input,
    head_value_input,
    decay_input_part,
    learning_rate_input,
    output_gate_input,
    decay_channel_offset,
    spike_log_decay,
    head_norm_gain,
    head_output_weight,
    projection_norm_gain,
    expert_input_rows,
    expert_norm_gain,
    selected_expert_index,
    selected_expert_weight,
    routed_gate_weight,
    routed_up_weight,
    routed_down_weight,
    common_gate_weight,
    common_up_weight,
    common_down_weight,
):
    attention_output = attention_mixer(
        receptance,
        head_key_input,
        head_value_input,
        decay_input_part,
        learning_rate_input,
        output_gate_input,
        decay_channel_offset,
        spike_log_decay,
        head_norm_gain,
        head_output_weight,
        projection_norm_gain,
    )
    expert_output = expert_half(
        expert_input_rows,
        expert_norm_gain,
        selected_expert_index,
        selected_expert_weight,
        routed_gate_weight,
        routed_up_weight,
        routed_down_weight,
        common_gate_weight,
        common_up_weight,
        common_down_weight,
    )
    return (attention_output, expert_output)


def solution(mesh):
    placed = (
        P("ep", "tp"),
        P("ep", "tp"),
        P("ep", "tp"),
        P("ep", "tp"),
        P("ep", "tp"),
        P("ep", "tp"),
        P("tp"),
        P("ep", "tp"),
        P("tp"),
        P("tp", None),
        P(),
        P("ep", None),
        P(),
        P("ep", None),
        P("ep", None),
        P(("ep", "tp"), None, None),
        P(("ep", "tp"), None, None),
        P(("ep", "tp"), None, None),
        P(None, "tp"),
        P(None, "tp"),
        P("tp", None),
    )
    return jax.shard_map(
        body,
        mesh=mesh,
        in_specs=placed,
        out_specs=(P(("ep", "tp"), None), P("ep", "tp")),
        check_vma=False,
    )
```

profile of v0, /device:TPU:1, one launch (start us, length us, event | category | flops | bytes accessed | tf_op | source)
XLA Modules:
  0.0 264.1 jit_solution(8176590577924353984)
XLA Ops:
  7.9 13.7 %all-to-all-start.2 = ((bf16[32,2,2048]{2,1,0:T(2,128)(2,1)}), bf16[32,2,2048]{2,1,0:T(2,128)(2,1)S(1)}, u32[]{:S(2)}, u32[]{:S(2)}) async-start(bf16[32,2,2048]{2,1,0:T(2,128)(2,1)} %broadcast_select_fusion.1), calls=%async_computation.2 | async-start | bytes 524288 | tf_op jit(solution)/shard_map/all_to_all | solution.py:237
  24.8 8.2 %all-to-all-done.2 = bf16[32,2,2048]{2,1,0:T(2,128)(2,1)S(1)} async-done(((bf16[32,2,2048]{2,1,0:T(2,128)(2,1)}), bf16[32,2,2048]{2,1,0:T(2,128)(2,1)S(1)}, u32[]{:S(2)}, u32[]{:S(2)}) %all-to-all-start.2) | async-done | bytes 262176 | tf_op jit(solution)/shard_map/all_to_all | solution.py:237
  36.6 11.4 %reduce.11 = bf16[2048,64]{1,0:T(8,128)(2,1)S(1)} reduce(bf16[2048,1,64]{2,1,0:T(2,128)(2,1)S(1)} %bitcast.416, bf16[]{:T(256)} %broadcast.542), dimensions={1}, to_apply=%bitcast.299.reduce_sub_computation | reduce | bytes 524290
  49.2 9.6 %all-to-all-start.3 = ((bf16[16,2,4096]{2,1,0:T(2,128)(2,1)}), bf16[16,2,4096]{2,1,0:T(2,128)(2,1)}, u32[]{:S(2)}, u32[]{:S(2)}) async-start(bf16[16,2,4096]{2,1,0:T(2,128)(2,1)} %reshape.866), calls=%async_computation.3 | async-start | bytes 524288 | tf_op jit(solution)/shard_map/all_to_all | solution.py:245
  58.8 110.0 %while.12 = (s32[]{:T(128)}, f32[1,128,64]{1,2,0:T(8,128)S(1)}, f32[4,1,64,128]{3,2,1,0:T(8,128)}, f32[4,1,64,64]{3,2,1,0:T(8,128)S(1)}, f32[4,1,64,64]{3,2,1,0:...) while((s32[]{:T(128)}, f32[1,128,64]{1,2,0:T(8,128)S(1)}, ...), condition=%wide.region_3.4_spmd, body=%wide.region_1.3_spmd.sunk | while | flops 18198592 | bytes 9869441 | solution.py:166
  62.0 3.3 %copy.318 = f32[64,64,64]{0,1,2:T(8,128)S(1)} copy(f32[64,64,64]{2,1,0:T(8,128)} %get-tuple-element.168) | data formatting | bytes 2097152 | tf_op jit(solution)/shard_map/while
  65.3 4.2 %copy.322 = f32[64,64,64]{0,1,2:T(8,128)} copy(f32[64,64,64]{2,1,0:T(8,128)} %get-tuple-element.172) | data formatting | bytes 2097152 | tf_op jit(solution)/shard_map/while
  74.8 4.9 %custom-call.10 = f32[1,64,64]{1,2,0:T(8,128)S(1)} custom-call(f32[1,64,64]{2,1,0:T(8,128)S(1)} %add_bitcast_fusion.2), custom_call_target="InvertDiagBlocksLowerTriangular" | custom-call | tf_op jit(solution)/shard_map/while/body/eval_jaxpr/jit(_solve_triangular)/triangular_solve | solution.py:105
  89.5 3.3 %copy.318 = f32[64,64,64]{0,1,2:T(8,128)S(1)} copy(f32[64,64,64]{2,1,0:T(8,128)} %get-tuple-element.168) | data formatting | bytes 2097152 | tf_op jit(solution)/shard_map/while
  92.8 4.2 %copy.322 = f32[64,64,64]{0,1,2:T(8,128)} copy(f32[64,64,64]{2,1,0:T(8,128)} %get-tuple-element.172) | data formatting | bytes 2097152 | tf_op jit(solution)/shard_map/while
  102.3 4.9 %custom-call.10 = f32[1,64,64]{1,2,0:T(8,128)S(1)} custom-call(f32[1,64,64]{2,1,0:T(8,128)S(1)} %add_bitcast_fusion.2), custom_call_target="InvertDiagBlocksLowerTriangular" | custom-call | tf_op jit(solution)/shard_map/while/body/eval_jaxpr/jit(_solve_triangular)/triangular_solve | solution.py:105
  117.0 3.3 %copy.318 = f32[64,64,64]{0,1,2:T(8,128)S(1)} copy(f32[64,64,64]{2,1,0:T(8,128)} %get-tuple-element.168) | data formatting | bytes 2097152 | tf_op jit(solution)/shard_map/while
  120.3 4.2 %copy.322 = f32[64,64,64]{0,1,2:T(8,128)} copy(f32[64,64,64]{2,1,0:T(8,128)} %get-tuple-element.172) | data formatting | bytes 2097152 | tf_op jit(solution)/shard_map/while
  129.8 4.9 %custom-call.10 = f32[1,64,64]{1,2,0:T(8,128)S(1)} custom-call(f32[1,64,64]{2,1,0:T(8,128)S(1)} %add_bitcast_fusion.2), custom_call_target="InvertDiagBlocksLowerTriangular" | custom-call | tf_op jit(solution)/shard_map/while/body/eval_jaxpr/jit(_solve_triangular)/triangular_solve | solution.py:105
  147.8 4.2 %copy.322 = f32[64,64,64]{0,1,2:T(8,128)} copy(f32[64,64,64]{2,1,0:T(8,128)} %get-tuple-element.172) | data formatting | bytes 2097152 | tf_op jit(solution)/shard_map/while
  157.3 4.9 %custom-call.10 = f32[1,64,64]{1,2,0:T(8,128)S(1)} custom-call(f32[1,64,64]{2,1,0:T(8,128)S(1)} %add_bitcast_fusion.2), custom_call_target="InvertDiagBlocksLowerTriangular" | custom-call | tf_op jit(solution)/shard_map/while/body/eval_jaxpr/jit(_solve_triangular)/triangular_solve | solution.py:105
  169.9 4.0 %all-to-all-start = ((bf16[32,128,64]{1,2,0:T(8,128)(2,1)}), bf16[32,128,64]{1,2,0:T(8,128)(2,1)S(1)}, u32[]{:S(2)}, u32[]{:S(2)}) async-start(bf16[32,128,64]{1,2,0:T(8,128)(2,1)} %broadcast_in_dim.111), calls=%async_computation | async-start | bytes 1048576 | tf_op jit(solution)/shard_map/all_to_all | solution.py:16
  181.7 8.9 %all-to-all-done = bf16[32,128,64]{1,2,0:T(8,128)(2,1)S(1)} async-done(((bf16[32,128,64]{1,2,0:T(8,128)(2,1)}), bf16[32,128,64]{1,2,0:T(8,128)(2,1)S(1)}, u32[]{:S(2)}, u32[]{:S(2)}) %all-to-all-start) | async-done | bytes 524320 | tf_op jit(solution)/shard_map/all_to_all | solution.py:16
  190.6 8.9 %all-to-all-start.5 = ((bf16[16,128,128]{1,2,0:T(8,128)(2,1)}), bf16[16,128,128]{1,2,0:T(8,128)(2,1)S(1)}, u32[]{:S(2)}, u32[]{:S(2)}) async-start(bf16[16,128,128]{1,2,0:T(8,128)(2,1)} %bitcast.340), calls=%async_computation.5 | async-start | bytes 1048576 | tf_op jit(solution)/shard_map/all_to_all | solution.py:69
  205.8 10.9 %all-to-all-done.5 = bf16[16,128,128]{1,2,0:T(8,128)(2,1)S(1)} async-done(((bf16[16,128,128]{1,2,0:T(8,128)(2,1)}), bf16[16,128,128]{1,2,0:T(8,128)(2,1)S(1)}, u32[]{:S(2)}, u32[]{:S(2)}) %all-to-all-start.5) | async-done | bytes 524320 | tf_op jit(solution)/shard_map/all_to_all | solution.py:69
  216.7 4.4 %all-to-all-start.4 = ((bf16[8,32,2,128]{3,2,0,1:T(2,128)(2,1)}), bf16[8,32,2,128]{3,2,0,1:T(2,128)(2,1)S(1)}, u32[]{:S(2)}, u32[]{:S(2)}) async-start(bf16[8,32,2,128]{3,2,0,1:T(2,128)(2,1)} %copy.262), calls=%async_computation.4 | async-start | bytes 262144 | tf_op jit(solution)/shard_map/all_to_all | solution.py:252
  222.6 8.8 %all-to-all-done.4 = bf16[8,32,2,128]{3,2,0,1:T(2,128)(2,1)S(1)} async-done(((bf16[8,32,2,128]{3,2,0,1:T(2,128)(2,1)}), bf16[8,32,2,128]{3,2,0,1:T(2,128)(2,1)S(1)}, u32[]{:S(2)}, u32[]{:S(2)}) %all-to-all-start.4) | async-done | bytes 131104 | tf_op jit(solution)/shard_map/all_to_all | solution.py:252
  231.4 3.7 %all-to-all-start.1 = ((bf16[16,16,2048]{2,1,0:T(8,128)(2,1)}), bf16[16,16,2048]{2,1,0:T(8,128)(2,1)S(1)}, u32[]{:S(2)}, u32[]{:S(2)}) async-start(bf16[16,16,2048]{2,1,0:T(8,128)(2,1)} %bitcast.90), calls=%async_computation.1 | async-start | bytes 2097152 | tf_op jit(solution)/shard_map/all_to_all | solution.py:69
  237.6 25.4 %all-to-all-done.1 = bf16[16,16,2048]{2,1,0:T(8,128)(2,1)S(1)} async-done(((bf16[16,16,2048]{2,1,0:T(8,128)(2,1)}), bf16[16,16,2048]{2,1,0:T(8,128)(2,1)S(1)}, u32[]{:S(2)}, u32[]{:S(2)}) %all-to-all-start.1) | async-done | bytes 1048608 | tf_op jit(solution)/shard_map/all_to_all | solution.py:69
  (259 shorter events, 98.2 us)
Async XLA Ops:
  0.6 32.7 %copy-start = (bf16[1,256,2048]{2,1,0:T(8,128)(2,1)S(1)}, bf16[1,256,2048]{2,1,0:T(8,128)(2,1)}, u32[]{:S(2)}) copy-start(bf16[1,256,2048]{2,1,0:T(8,128)(2,1)} %param.40) | copy-start | bytes 3145732
  5.6 16.3 %copy-start.1 = (bf16[128,2048]{1,0:T(8,128)(2,1)}, bf16[128,2048]{1,0:T(8,128)(2,1)S(1)}, u32[]{:S(2)}) copy-start(bf16[128,2048]{1,0:T(8,128)(2,1)S(1)} %fusion.58) | copy-start | bytes 1572868
  5.6 16.1 %copy-start.11 = (bf16[256,64]{0,1:T(8,128)(2,1)S(1)}, bf16[256,64]{0,1:T(8,128)(2,1)}, u32[]{:S(2)}) copy-start(bf16[256,64]{0,1:T(8,128)(2,1)} %param.24) | copy-start | bytes 98308
  5.6 16.1 %copy-start.12 = (f32[256,64]{0,1:T(8,128)S(1)}, f32[256,64]{0,1:T(8,128)}, u32[]{:S(2)}) copy-start(f32[256,64]{0,1:T(8,128)} %param.30) | copy-start | bytes 196612
  5.6 16.1 %copy-start.14 = (bf16[256,64]{0,1:T(8,128)(2,1)S(1)}, bf16[256,64]{0,1:T(8,128)(2,1)}, u32[]{:S(2)}) copy-start(bf16[256,64]{0,1:T(8,128)(2,1)} %param.26) | copy-start | bytes 98308
  5.6 16.1 %copy-start.26 = (f32[64]{0:T(128)S(1)}, f32[64]{0:T(128)}, u32[]{:S(2)}) copy-start(f32[64]{0:T(128)} %param.29) | copy-start | bytes 772
  5.6 16.7 %copy-start.15 = (bf16[256,64]{0,1:T(8,128)(2,1)S(1)}, bf16[256,64]{0,1:T(8,128)(2,1)}, u32[]{:S(2)}) copy-start(bf16[256,64]{0,1:T(8,128)(2,1)} %param.23) | copy-start | bytes 98308
  5.6 17.4 %copy-start.16 = (bf16[256,64]{0,1:T(8,128)(2,1)S(1)}, bf16[256,64]{0,1:T(8,128)(2,1)}, u32[]{:S(2)}) copy-start(bf16[256,64]{0,1:T(8,128)(2,1)} %param.25) | copy-start | bytes 98308
  6.4 26.6 %copy-start.6 = (bf16[1,2048,256]{2,1,0:T(8,128)(2,1)S(1)}, bf16[1,2048,256]{2,1,0:T(8,128)(2,1)}, u32[]{:S(2)}) copy-start(bf16[1,2048,256]{2,1,0:T(8,128)(2,1)} %param.38) | copy-start | bytes 3145732
  7.9 25.0 %all-to-all-start.2 = ((bf16[32,2,2048]{2,1,0:T(2,128)(2,1)}), bf16[32,2,2048]{2,1,0:T(2,128)(2,1)S(1)}, u32[]{:S(2)}, u32[]{:S(2)}) async-start(bf16[32,2,2048]{2,1,0:T(2,128)(2,1)} %broadcast_select_fusion.1), calls=%async_computation.2 | async-start | bytes 524288 | tf_op jit(solution)/shard_map/all_to_all | solution.py:237
  49.2 119.8 %all-to-all-start.3 = ((bf16[16,2,4096]{2,1,0:T(2,128)(2,1)}), bf16[16,2,4096]{2,1,0:T(2,128)(2,1)}, u32[]{:S(2)}, u32[]{:S(2)}) async-start(bf16[16,2,4096]{2,1,0:T(2,128)(2,1)} %reshape.866), calls=%async_computation.3 | async-start | bytes 524288 | tf_op jit(solution)/shard_map/all_to_all | solution.py:245
  169.9 20.7 %all-to-all-start = ((bf16[32,128,64]{1,2,0:T(8,128)(2,1)}), bf16[32,128,64]{1,2,0:T(8,128)(2,1)S(1)}, u32[]{:S(2)}, u32[]{:S(2)}) async-start(bf16[32,128,64]{1,2,0:T(8,128)(2,1)} %broadcast_in_dim.111), calls=%async_computation | async-start | bytes 1048576 | tf_op jit(solution)/shard_map/all_to_all | solution.py:16
  190.6 26.1 %all-to-all-start.5 = ((bf16[16,128,128]{1,2,0:T(8,128)(2,1)}), bf16[16,128,128]{1,2,0:T(8,128)(2,1)S(1)}, u32[]{:S(2)}, u32[]{:S(2)}) async-start(bf16[16,128,128]{1,2,0:T(8,128)(2,1)} %bitcast.340), calls=%async_computation.5 | async-start | bytes 1048576 | tf_op jit(solution)/shard_map/all_to_all | solution.py:69
  203.9 17.1 %copy-start.10 = (bf16[64,2048]{1,0:T(8,128)(2,1)S(1)}, bf16[64,2048]{1,0:T(8,128)(2,1)}, u32[]{:S(2)}) copy-start(bf16[64,2048]{1,0:T(8,128)(2,1)} %param.32) | copy-start | bytes 786436
  204.0 17.1 %copy-start.17 = (bf16[256,64]{0,1:T(8,128)(2,1)S(1)}, bf16[256,64]{0,1:T(8,128)(2,1)}, u32[]{:S(2)}) copy-start(bf16[256,64]{0,1:T(8,128)(2,1)} %param.28) | copy-start | bytes 98308
  204.0 17.1 %copy-start.25 = (f32[64]{0:T(128)S(1)}, f32[64]{0:T(128)}, u32[]{:S(2)}) copy-start(f32[64]{0:T(128)} %param.31) | copy-start | bytes 772
  205.5 29.6 %copy-start.19 = (s32[256]{0:T(256)S(1)}, s32[256]{0:T(256)}, u32[]{:S(2)}) copy-start(s32[256]{0:T(256)} %copy-done.18) | copy-start | bytes 3076
  205.5 29.7 %copy-start.23 = (s32[128,2]{0,1:T(2,128)S(1)}, s32[128,2]{0,1:T(2,128)}, u32[]{:S(2)}) copy-start(s32[128,2]{0,1:T(2,128)} %param.36) | copy-start | bytes 3076
  205.5 29.9 %copy-start.24 = (f32[128,2]{0,1:T(2,128)S(1)}, f32[128,2]{0,1:T(2,128)}, u32[]{:S(2)}) copy-start(f32[128,2]{0,1:T(2,128)} %param.37) | copy-start | bytes 3076
  205.6 29.9 %copy-start.22 = (s32[256,1]{0,1:T(1,128)S(1)}, s32[256,1]{0,1:T(1,128)}, u32[]{:S(2)}) copy-start(s32[256,1]{0,1:T(1,128)} %get-tuple-element.93) | copy-start | bytes 3076
  205.6 29.9 %copy-start.5 = (s32[128,2]{1,0:T(8,128)S(1)}, s32[128,2]{1,0:T(8,128)}, u32[]{:S(2)}) copy-start(s32[128,2]{1,0:T(8,128)} %copy-done.4) | copy-start | bytes 3076
  216.7 14.7 %all-to-all-start.4 = ((bf16[8,32,2,128]{3,2,0,1:T(2,128)(2,1)}), bf16[8,32,2,128]{3,2,0,1:T(2,128)(2,1)S(1)}, u32[]{:S(2)}, u32[]{:S(2)}) async-start(bf16[8,32,2,128]{3,2,0,1:T(2,128)(2,1)} %copy.262), calls=%async_computation.4 | async-start | bytes 262144 | tf_op jit(solution)/shard_map/all_to_all | solution.py:252
  231.4 31.7 %all-to-all-start.1 = ((bf16[16,16,2048]{2,1,0:T(8,128)(2,1)}), bf16[16,16,2048]{2,1,0:T(8,128)(2,1)S(1)}, u32[]{:S(2)}, u32[]{:S(2)}) async-start(bf16[16,16,2048]{2,1,0:T(8,128)(2,1)} %bitcast.90), calls=%async_computation.1 | async-start | bytes 2097152 | tf_op jit(solution)/shard_map/all_to_all | solution.py:69
  235.1 28.3 %copy-start.21 = (f32[2048]{0:T(1024)S(1)}, f32[2048]{0:T(1024)}, u32[]{:S(2)}) copy-start(f32[2048]{0:T(1024)} %param.33) | copy-start | bytes 24580
  (9 other events, 58.7 us)
where the time goes:
time: 267 us; the launch traced here: 264 us
  other arithmetic  68.4 us (26%)
  waiting for transfers between devices  62.2 us (23%)
  local copies, waits for them, and re-layouts  53.6 us (20%)
  starting transfers between devices  44.2 us (17%)
  matrix products  33.9 us (13%)
    all_to_all x2, waiting for transfers between devices, sent_and_summed(): blocks = lax.all_to_all(in_blocks(x, dim, size), axis, 0, 0, tiled=True)  36.3 us
    while x8, local copies, waits for them, and re-layouts  30 us
    another operation x12, other arithmetic, within_block(): jax.scipy.linalg.solve_triangular(identity - lower_beta, right_side, lowe...  19.9 us
    all_to_all x1, starting transfers between devices, expert_half(): lax.all_to_all(outgoing, 'ep', split_axis=0, concat_axis=0, tiled=True)  13.7 us
    while x4, other arithmetic  12.9 us
    all_to_all x2, starting transfers between devices, sent_and_summed(): blocks = lax.all_to_all(in_blocks(x, dim, size), axis, 0, 0, tiled=True)  12.6 us
    exp x4, other arithmetic, within_block(): jnp.exp(jnp.where(inclusive, cumul[:, :, None, :] - cumul[:, None, :, :],...  12.3 us
    unnamed x2, other arithmetic  11.5 us
  transfers between devices with their start and end apart: 6, of which 5 were waited for; matrix products, arithmetic and copies ran while one was open for 49% of the time, Pallas kernels for 0%

commit v1 on v0

v1 whole, which is shorter than its diff:
```python
import functools
import math

import jax
import jax.numpy as jnp
from jax import lax
from jax.experimental import pallas as pl
from jax.experimental.pallas import tpu as pltpu
from jax.sharding import PartitionSpec as P

HC = 64
L = 128
GROUPS = 8
CAP = 2
NORM_EPSILON = 1e-06
GROUP_EPSILON = 0.00064
F32 = jnp.float32
BF16 = jnp.bfloat16
MESH = pl.DeviceIdType.MESH


def nn(a, b):
    return jnp.dot(a, b, preferred_element_type=F32)


def nt(a, b):
    return lax.dot_general(a, b, (((1,), (1,)), ((), ())), preferred_element_type=F32)


def parts(a, count):
    out = []
    for k in range(count):
        piece = a.astype(BF16)
        out.append(piece)
        if k < count - 1:
            a = a - piece.astype(F32)
    return out


def mm(a, b, product=nn, na=2, nb=2):
    pa = [a] if a.dtype == BF16 else parts(a, na)
    pb = [b] if b.dtype == BF16 else parts(b, nb)
    total = None
    for i, x in enumerate(pa):
        for j, y in enumerate(pb):
            if i + j < max(len(pa), len(pb)):
                term = product(x, y)
                total = term if total is None else total + term
    return total


def iota(shape, dim):
    return lax.broadcasted_iota(jnp.int32, shape, dim)


def sigmoid(v):
    return 1.0 / (1.0 + jnp.exp(-v))


def column(row):
    n = row.shape[1]
    return jnp.sum(
        jnp.where(iota((n, n), 0) == iota((n, n), 1), row, 0.0), axis=1, keepdims=True
    )


def beside_identity(f):
    top = jnp.where(iota((HC, 2 * HC), 0) == iota((HC, 2 * HC), 1), 1.0, 0.0)
    return jnp.concatenate([top.astype(f.dtype), f], axis=0)


def joined(late, early):
    return mm(late, beside_identity(early))


def block_inverse(n):
    r, c = iota((L, L), 0), iota((L, L), 1)
    eye = jnp.where(r == c, 1.0, 0.0)
    small = jnp.where(r // 8 == c // 8, n, 0.0)
    two = mm(small, small)
    four = mm(two, two)
    first = eye + small + two + mm(small, two)
    x = first + mm(first, four)
    size = 8
    while size < L:
        lower, upper = r // size, c // size
        off = jnp.where((upper == lower + 1) & (lax.rem(lower, 2) == 0), n, 0.0)
        x = x + mm(mm(x, off), x)
        size *= 2
    return x


def local_block(rec, key, val, removal, lr, ld):
    s, t = iota((L, L), 0), iota((L, L), 1)
    upto = jnp.where(s <= t, 1.0, 0.0).astype(BF16)
    cum = sum(nn(p, upto) for p in parts(ld, 3))
    ref, end = cum[:, L // 2 - 1 : L // 2], cum[:, L - 1 : L]
    eq = jnp.exp(cum - ref)
    eb = jnp.exp(cum - ld - ref)
    ek = jnp.exp(ref - cum)
    eref, eend = jnp.exp(ref), jnp.exp(end - ref)
    qn, qr = -removal * eb, rec * eq
    kb, kk = removal * lr * ek, key * lr * ek
    keys = jnp.concatenate([kb.T, kk.T], axis=0)
    both = mm(keys, jnp.concatenate([qn, qr], axis=1))
    lb = jnp.where(s < t, both[:L, :L], 0.0)
    ob = jnp.where(s <= t, both[:L, L:], 0.0)
    lk = jnp.where(s < t, both[L:, :L], 0.0)
    ok = jnp.where(s <= t, both[L:, L:], 0.0)
    valued = mm(val, jnp.concatenate([lk, ok], axis=1))
    right = jnp.concatenate([valued[:, :L], qn * eref], axis=0)
    corr = mm(right, block_inverse(lb))
    z = mm(corr, ob) + jnp.concatenate([valued[:, L:], qr * eref], axis=0)
    aug = jnp.concatenate([val, jnp.zeros_like(val)], axis=0)
    f = mm(
        jnp.concatenate([kb * eend, kk * eend], axis=1),
        jnp.concatenate([corr, aug.astype(F32)], axis=1),
        nt,
    )
    f = f + jnp.where(
        iota((HC, 2 * HC), 0) + HC == iota((HC, 2 * HC), 1), jnp.exp(end), 0.0
    )
    return f, z


def kernel(nx, nz, *refs):
    (rec, key, val, dec, lrn, gat, spk, dco, hng, png, eng, idx, wts) = refs[:13]
    (how_h, exr_h, rg_h, ru_h, rd_h, cg_h, cu_h, cd_h) = refs[13:21]
    out_a, out_b = refs[21:23]
    (how, exr, rg, ru, rd, cgu, cd, nb, dout, darr, ep, epr, es, rb, rout, rarr,
     sp, spr, ss, sb, ap, apr, aps, ab, xarr, zs, zarr, load, pair_s, pair_r, dsend, drecv,
     ysend, yrecv, rsend, rrecv, xsend, xrecv, zsend, zrecv) = refs[23:]
    n_ep = nx * nz
    tb = exr.shape[0]
    rows = n_ep * CAP
    slots = rows * GROUPS
    me, t = lax.axis_index("ep"), lax.axis_index("tp")
    y, c = lax.div(t, 2), lax.rem(t, 2)
    z, x = lax.div(me, nx), lax.rem(me, nx)
    other = t + 1 - 2 * c

    def remote(src, dst, send, recv, where):
        return pltpu.make_async_remote_copy(
            src_ref=src, dst_ref=dst, send_sem=send, recv_sem=recv,
            device_id=where, device_id_type=MESH,
        )

    def drain(ref, sem):
        pltpu.make_async_copy(ref, ref, sem).wait()

    loads = [
        pltpu.make_async_copy(a, b, load.at[k])
        for k, (a, b) in enumerate((
            (exr_h, exr), (cg_h, cgu.at[0:HC]), (cu_h, cgu.at[HC : 2 * HC]), (cd_h, cd),
            (rg_h, rg), (ru_h, ru), (rd_h, rd), (how_h, how),
        ))
    ]
    for copy in loads:
        copy.start()

    unit = jnp.where(iota((HC, 2 * HC), 0) + HC == iota((HC, 2 * HC), 1), 1.0, 0.0)
    for k in range(nz):
        zarr[k] = unit.astype(BF16)

    barrier = pltpu.get_barrier_semaphore()
    pl.semaphore_signal(barrier, inc=1, device_id={"tp": other}, device_id_type=MESH)
    for d in range(1, GROUPS):
        pl.semaphore_signal(
            barrier, inc=1, device_id={"tp": 2 * lax.rem(y + d, GROUPS) + c}, device_id_type=MESH
        )

    def greet(d, carry):
        pl.semaphore_signal(
            barrier, inc=1, device_id={"ep": lax.rem(me + d, n_ep)}, device_id_type=MESH
        )
        return carry

    lax.fori_loop(1, n_ep, greet, 0)

    loads[0].wait()
    wide = exr[...].astype(F32)
    scale = lax.rsqrt(jnp.mean(wide * wide, axis=1, keepdims=True) + NORM_EPSILON)
    nb[...] = (wide * scale * eng[...]).astype(BF16)

    width = nb.shape[1] // GROUPS
    first, second = idx[0:1, :], idx[1:2, :]
    i = iota((slots, tb), 0)
    expert = lax.div(i, 16) * GROUPS + y
    hits = jnp.where((first == expert) | (second == expert), 1.0, 0.0)
    earlier = jnp.where(iota((tb, tb), 0) < iota((tb, tb), 1), 1.0, 0.0).astype(BF16)
    rank = nn(hits.astype(BF16), earlier)
    mine = jnp.where(rank == lax.rem(lax.div(i, 8), 2).astype(F32), hits, 0.0)
    piece = lax.rem(i, 8)
    picks = jnp.concatenate(
        [jnp.where(piece == j, mine, 0.0).astype(BF16) for j in range(GROUPS)], axis=1
    )
    stacked = jnp.concatenate(
        [nb[:, j * width : (j + 1) * width] for j in range(GROUPS)], axis=0
    )
    dout[...] = nn(picks, stacked).astype(BF16)
    own = pl.ds(pl.multiple_of(me * 16, 16), 16)
    darr[own, :] = dout[own, :]

    loads[1].wait()
    loads[2].wait()
    loads[3].wait()
    gate_up = nt(cgu[...], nb[...])
    g, u = gate_up[:HC], gate_up[HC:]
    hidden = (g * sigmoid(g) * u).T.astype(BF16)
    shared = nn(hidden, cd[...]).astype(BF16)
    cols = shared.shape[1] // (2 * GROUPS)
    for k in range(2 * GROUPS):
        sp[k % 2, k // 2] = shared[:, k * cols : (k + 1) * cols]

    pl.semaphore_wait(barrier, GROUPS + n_ep - 1)

    def send_rows(d, carry):
        to = lax.rem(me + d, n_ep)
        remote(
            dout.at[pl.ds(pl.multiple_of(to * 16, 16), 16)], darr.at[own],
            dsend, drecv, {"ep": to},
        ).start()
        return carry

    lax.fori_loop(1, n_ep, send_rows, 0)
    pair_shared = remote(sp.at[1 - c], spr, pair_s.at[0], pair_r.at[0], {"tp": other})
    pair_shared.start()

    k_in = key[...].astype(F32)
    pre = column(dco[...]) + jnp.tanh(dec[...].astype(F32))
    ld = spk[...] - sigmoid(pre) * math.exp(-0.5)
    lr = sigmoid(lrn[...].astype(F32))
    removal = k_in * lax.rsqrt(jnp.sum(k_in * k_in, axis=0, keepdims=True) + NORM_EPSILON)
    r_in = rec[...].astype(F32)
    blocks = []
    for b in range(key.shape[1] // L):
        at = slice(b * L, (b + 1) * L)
        blocks.append(
            local_block(r_in[:, at], k_in[:, at], val[:, at], removal[:, at], lr[:, at], ld[:, at])
        )
    f, z_out = blocks[0]
    z_all = [z_out]
    for later_f, later_z in blocks[1:]:
        z_all.append(mm(beside_identity(f).T, later_z))
        f = joined(later_f, f)
    z_all = jnp.concatenate(z_all, axis=1)
    xarr[x] = f.astype(BF16)
    x_sends = [
        remote(
            xarr.at[x], xarr.at[x], xsend.at[d - 1], xrecv.at[d - 1],
            {"ep": z * nx + lax.rem(x + d, nx)},
        )
        for d in range(1, nx)
    ]
    for copy in x_sends:
        copy.start()

    pair_shared.wait()
    ss[...] = (sp[c].astype(F32) + spr[...].astype(F32)).astype(BF16)
    sb[y] = ss[y]
    y_sends = []
    for d in range(1, GROUPS):
        to = lax.rem(y + d, GROUPS)
        y_sends.append(
            remote(ss.at[to], sb.at[y], ysend.at[0, d - 1], yrecv.at[0, d - 1], {"tp": 2 * to + c})
        )
        y_sends[-1].start()

    drain(darr.at[0 : (n_ep - 1) * 16], drecv)
    r, q = iota((slots, slots), 0), iota((slots, slots), 1)
    source = lax.rem(r, n_ep) * 16 + lax.rem(lax.div(r, n_ep), 2) * 8 + lax.div(r, rows)
    turned = nn(jnp.where(q == source, 1.0, 0.0).astype(BF16), darr[...]).astype(BF16)
    rows_in = jnp.concatenate(
        [turned[j * rows : (j + 1) * rows] for j in range(GROUPS)], axis=1
    )
    loads[4].wait()
    loads[5].wait()
    g, u = nn(rows_in, rg[...]), nn(rows_in, ru[...])
    hidden = (g * sigmoid(g) * u).astype(BF16)
    loads[6].wait()
    routed = nn(hidden, rd[...]).astype(BF16)
    for k in range(2 * GROUPS):
        ep[k % 2, k // 2] = routed[:, k * cols : (k + 1) * cols]
    pair_routed = remote(ep.at[1 - c], epr, pair_s.at[1], pair_r.at[1], {"tp": other})
    pair_routed.start()

    for copy in x_sends:
        copy.wait()
    stretch = [xarr[k] for k in range(nx)]
    before = unit
    total = stretch[0]
    for k in range(1, nx):
        before = jnp.where(x == k, total.astype(F32), before)
        total = joined(stretch[k], total)
    zs[...] = total.astype(BF16)
    for d in range(1, nz):
        @pl.when(z + d < nz)
        def _():
            remote(
                zs, zarr.at[z], zsend.at[d - 1], zrecv.at[z], {"ep": (z + d) * nx + x}
            ).start()

    pair_routed.wait()
    es[...] = (ep[c].astype(F32) + epr[...].astype(F32)).astype(BF16)
    rb[y] = es[y]
    for d in range(1, GROUPS):
        to = lax.rem(y + d, GROUPS)
        y_sends.append(
            remote(es.at[to], rb.at[y], ysend.at[1, d - 1], yrecv.at[1, d - 1], {"tp": 2 * to + c})
        )
        y_sends[-1].start()
    z_all = mm(beside_identity(before).T, z_all)

    q = iota((slots, slots), 1)
    r = iota((slots, slots), 0)
    source = lax.div(lax.rem(r, 16), 2) * rows + lax.rem(r, 2) * n_ep + lax.div(r, 16)
    back = jnp.where(q == source, 1.0, 0.0).astype(BF16)
    lines = jnp.concatenate(
        [first.astype(F32), second.astype(F32), wts[...], jnp.zeros((4, tb), F32)], axis=0
    ).T
    q = iota((tb, slots), 1)
    expert = (lax.div(q, 16) * GROUPS + lax.div(lax.rem(q, 16), 2)).astype(F32)
    hit_a = jnp.where(lines[:, 0:1] == expert, 1.0, 0.0)
    hit_b = jnp.where(lines[:, 1:2] == expert, 1.0, 0.0)
    earlier = jnp.where(iota((tb, tb), 0) > iota((tb, tb), 1), 1.0, 0.0).astype(BF16)
    rank = nn(earlier, (hit_a + hit_b).astype(BF16))
    weight = jnp.where(
        rank == lax.rem(q, 2).astype(F32), hit_a * lines[:, 2:3] + hit_b * lines[:, 3:4], 0.0
    )

    for copy in y_sends[GROUPS - 1 :]:
        copy.wait()
    every = jnp.concatenate([rb[k] for k in range(GROUPS)], axis=0)
    rout[...] = nn(back, every).astype(BF16)
    rarr[own, :] = rout[own, :]

    def send_back(d, carry):
        to = lax.rem(me + d, n_ep)
        remote(
            rout.at[pl.ds(pl.multiple_of(to * 16, 16), 16)], rarr.at[own],
            rsend, rrecv, {"ep": to},
        ).start()
        return carry

    lax.fori_loop(1, n_ep, send_back, 0)

    for k in range(nz - 1):
        @pl.when(k < z)
        def _():
            drain(zarr.at[k], zrecv.at[k])

    level = [zarr[k] for k in range(nz - 1)] if nz > 1 else [unit.astype(BF16)]
    while len(level) > 1:
        nxt = [joined(level[k + 1], level[k]) for k in range(0, len(level) - 1, 2)]
        if len(level) % 2:
            nxt.append(level[-1].astype(F32))
        level = nxt
    carried = level[0].astype(F32)
    head = mm(beside_identity(carried).T[:HC], z_all)
    centred = head - jnp.mean(head, axis=0, keepdims=True)
    normed = centred * lax.rsqrt(jnp.mean(centred * centred, axis=0, keepdims=True) + GROUP_EPSILON)
    heads_out = normed * column(hng[...]) * sigmoid(gat[...].astype(F32))
    heads_out = heads_out.T.astype(BF16)
    loads[7].wait()
    mixed = nn(heads_out, how[...]).astype(BF16)
    own_rows = out_a.shape[0]
    for k in range(2 * GROUPS):
        ap[k % 2, k // 2] = mixed[k * own_rows : (k + 1) * own_rows]
    pair_mix = remote(ap.at[1 - c], apr, pair_s.at[2], pair_r.at[2], {"tp": other})
    pair_mix.start()
    pair_mix.wait()
    aps[...] = (ap[c].astype(F32) + apr[...].astype(F32)).astype(BF16)
    ab[y] = aps[y]
    a_sends = []
    for d in range(1, GROUPS):
        to = lax.rem(y + d, GROUPS)
        a_sends.append(
            remote(aps.at[to], ab.at[y], ysend.at[2, d - 1], yrecv.at[2, d - 1], {"tp": 2 * to + c})
        )
        a_sends[-1].start()

    for copy in y_sends[: GROUPS - 1]:
        copy.wait()
    drain(rarr.at[0 : (n_ep - 1) * 16], rrecv)
    answer = mm(weight, rarr[...])
    for k in range(GROUPS):
        answer = answer + sb[k].astype(F32)
    out_b[...] = answer.astype(BF16)

    for copy in a_sends:
        copy.wait()
    mix = ab[0].astype(F32)
    for k in range(1, GROUPS):
        mix = mix + ab[k].astype(F32)
    scale = lax.rsqrt(jnp.mean(mix * mix, axis=1, keepdims=True) + NORM_EPSILON)
    out_a[...] = (mix * scale * png[...]).astype(BF16)

    for d in range(1, nz):
        @pl.when(z + d < nz)
        def _():
            drain(zs, zsend.at[d - 1])
    drain(dout.at[0 : (n_ep - 1) * 16], dsend)
    drain(rout.at[0 : (n_ep - 1) * 16], rsend)


def solution(mesh):
    n_ep = mesh.shape["ep"]
    nx = 4 if n_ep % 4 == 0 else n_ep
    nz = n_ep // nx

    def body(rec, key, val, dec, lrn, gat, dco, spk, hng, how, png, exr, eng, idx, wts,
             rg, ru, rd, cg, cu, cd):
        ta, d = rec.shape[0], how.shape[1]
        tb = exr.shape[0]
        own, cols = ta // (2 * GROUPS), d // (2 * GROUPS)
        rows = n_ep * CAP
        width = d // GROUPS
        small = [a.T for a in (rec, key, val, dec, lrn, gat, spk)]
        small += [a.reshape(1, -1) for a in (dco, hng, png, eng)] + [idx.T, wts.T]
        large = [how, exr, rg[0], ru[0], rd[0], cg.T, cu.T, cd]
        vmem = pl.BlockSpec(memory_space=pltpu.VMEM)
        dma = pltpu.SemaphoreType.DMA
        return pl.pallas_call(
            functools.partial(kernel, nx, nz),
            out_shape=(
                jax.ShapeDtypeStruct((own, d), BF16),
                jax.ShapeDtypeStruct((tb, cols), BF16),
            ),
            in_specs=[vmem] * len(small) + [pl.BlockSpec(memory_space=pl.ANY)] * len(large),
            out_specs=(vmem, vmem),
            scratch_shapes=[
                pltpu.VMEM(how.shape, BF16),
                pltpu.VMEM(exr.shape, BF16),
                pltpu.VMEM(rg.shape[1:], BF16),
                pltpu.VMEM(ru.shape[1:], BF16),
                pltpu.VMEM(rd.shape[1:], BF16),
                pltpu.VMEM((2 * HC, d), BF16),
                pltpu.VMEM(cd.shape, BF16),
                pltpu.VMEM((tb, d), BF16),
                pltpu.VMEM((n_ep * 16, width), BF16),
                pltpu.VMEM((n_ep * 16, width), BF16),
                pltpu.VMEM((2, GROUPS, rows, cols), BF16),
                pltpu.VMEM((GROUPS, rows, cols), BF16),
                pltpu.VMEM((GROUPS, rows, cols), BF16),
                pltpu.VMEM((GROUPS, rows, cols), BF16),
                pltpu.VMEM((n_ep * 16, cols), BF16),
                pltpu.VMEM((n_ep * 16, cols), BF16),
                pltpu.VMEM((2, GROUPS, tb, cols), BF16),
                pltpu.VMEM((GROUPS, tb, cols), BF16),
                pltpu.VMEM((GROUPS, tb, cols), BF16),
                pltpu.VMEM((GROUPS, tb, cols), BF16),
                pltpu.VMEM((2, GROUPS, own, d), BF16),
                pltpu.VMEM((GROUPS, own, d), BF16),
                pltpu.VMEM((GROUPS, own, d), BF16),
                pltpu.VMEM((GROUPS, own, d), BF16),
                pltpu.VMEM((nx, HC, 2 * HC), BF16),
                pltpu.VMEM((HC, 2 * HC), BF16),
                pltpu.VMEM((nz, HC, 2 * HC), BF16),
                dma((8,)),
                dma((3,)),
                dma((3,)),
                dma,
                dma,
                dma((3, GROUPS - 1)),
                dma((3, GROUPS - 1)),
                dma,
                dma,
                dma((max(nx - 1, 1),)),
                dma((max(nx - 1, 1),)),
                dma((max(nz - 1, 1),)),
                dma((max(nz, 1),)),
            ],
            compiler_params=pltpu.CompilerParams(
                collective_id=0, has_side_effects=True, vmem_limit_bytes=48 * 1024 * 1024
            ),
        )(*small, *large)

    placed = (
        P("ep", "tp"), P("ep", "tp"), P("ep", "tp"), P("ep", "tp"), P("ep", "tp"), P("ep", "tp"),
        P("tp"), P("ep", "tp"), P("tp"), P("tp", None), P(), P("ep", None), P(), P("ep", None),
        P("ep", None), P(("ep", "tp"), None, None), P(("ep", "tp"), None, None),
        P(("ep", "tp"), None, None), P(None, "tp"), P(None, "tp"), P("tp", None),
    )
    return jax.shard_map(
        body,
        mesh=mesh,
        in_specs=placed,
        out_specs=(P(("ep", "tp"), None), P("ep", "tp")),
        check_vma=False,
    )
```

time: 267 us -> 74 us (0.28)
  other arithmetic: 68.4 us -> 0 us
  waiting for transfers between devices: 62.2 us -> 0 us
  Pallas kernels: 0 us -> 54.5 us
  starting transfers between devices: 44.2 us -> 0 us
  local copies, waits for them, and re-layouts: 53.6 us -> 17.8 us
  matrix products: 33.9 us -> 0 us
    all_to_all x6 -> x0, waiting for transfers between devices: 62.2 us -> none  [the longest x2 36.3 us: sent_and_summed(): blocks = lax.all_to_all(in_blocks(x, dim, size), axis, 0, 0, tiled=True)]
    pallas_call x0 -> x1, Pallas kernels: none -> 54.5 us  [body(): pl.pallas_call(functools.partial(kernel, nx, nz), out_shape=(jax.ShapeDty...]
    all_to_all x6 -> x0, starting transfers between devices: 44.2 us -> none  [the longest x1 13.7 us: expert_half(): lax.all_to_all(outgoing, 'ep', split_axis=0, concat_axis=0, tiled=True)]
    dot_general x41 -> x0, matrix products: 32.8 us -> none  [the longest x4 5.99 us: within_block(): output = output + jnp.einsum('hts,hsr->htr', output_key, value_aug)]
    while x9 -> x0, local copies, waits for them, and re-layouts: 30.1 us -> none
    another operation x24 -> x0, other arithmetic: 23.7 us -> none  [the longest x12 19.9 us: within_block(): jax.scipy.linalg.solve_triangular(identity - lower_beta, right_side, lowe...]
    while x4 -> x0, other arithmetic: 12.9 us -> none
    exp x4 -> x0, other arithmetic: 12.3 us -> none  [within_block(): jnp.exp(jnp.where(inclusive, cumul[:, :, None, :] - cumul[:, None, :, :],...]
  transfers between devices with their start and end apart: 6 -> 0, of which waited for: 5 -> 0; matrix products, arithmetic and copies ran while one was open for 49% -> 0% of each run, Pallas kernels for 0% -> 0%
where the time goes in v1:
time: 74 us; the launch traced here: 73.1 us
  Pallas kernels  54.5 us (74%)
  local copies, waits for them, and re-layouts  17.8 us (24%)
    pallas_call x1, Pallas kernels, body(): pl.pallas_call(functools.partial(kernel, nx, nz), out_shape=(jax.ShapeDty...  54.5 us
    unnamed x44, local copies, waits for them, and re-layouts  17.8 us

profile of v1, /device:TPU:1, one launch (start us, length us, event | category | flops | bytes accessed | tf_op | source)
XLA Modules:
  0.0 73.1 jit_solution(15182982593704281569)
XLA Ops:
  0.6 0.0 copy-start.9
  0.6 0.0 copy-start.18
  0.7 0.7 copy-done.9
  1.4 1.2 %copy-done = bf16[1,2048,256]{2,1,0:T(8,128)(2,1)S(1)} copy-done((bf16[1,2048,256]{2,1,0:T(8,128)(2,1)S(1)}, bf16[1,2048,256]{2,1,0:T(8,128)(2,1)}, u32[]{:S(2)}) %copy-start) | copy-done | bytes 1048600
  2.6 1.2 %copy-done.1 = bf16[1,2048,256]{2,1,0:T(8,128)(2,1)S(1)} copy-done((bf16[1,2048,256]{2,1,0:T(8,128)(2,1)S(1)}, bf16[1,2048,256]{2,1,0:T(8,128)(2,1)}, u32[]{:S(2)}) %copy-start.1) | copy-done | bytes 1048600
  3.9 1.2 %copy-done.2 = bf16[1,256,2048]{2,1,0:T(8,128)(2,1)S(1)} copy-done((bf16[1,256,2048]{2,1,0:T(8,128)(2,1)S(1)}, bf16[1,256,2048]{2,1,0:T(8,128)(2,1)}, u32[]{:S(2)}) %copy-start.2) | copy-done | bytes 1048600
  5.1 1.0 %copy-done.3 = bf16[128,2048]{1,0:T(8,128)(2,1)S(1)} copy-done((bf16[128,2048]{1,0:T(8,128)(2,1)S(1)}, bf16[128,2048]{1,0:T(8,128)(2,1)}, u32[]{:S(2)}) %copy-start.3) | copy-done | bytes 524312
  6.1 0.9 %copy-done.4 = bf16[64,2048]{1,0:T(8,128)(2,1)S(1)} copy-done((bf16[64,2048]{1,0:T(8,128)(2,1)S(1)}, bf16[64,2048]{1,0:T(8,128)(2,1)}, u32[]{:S(2)}) %copy-start.4) | copy-done | bytes 262168
  7.1 0.9 %copy-done.5 = bf16[2048,64]{0,1:T(8,128)(2,1)S(1)} copy-done((bf16[2048,64]{0,1:T(8,128)(2,1)S(1)}, bf16[2048,64]{0,1:T(8,128)(2,1)}, u32[]{:S(2)}) %copy-start.5) | copy-done | bytes 262168
  8.0 0.9 %copy-done.6 = bf16[2048,64]{0,1:T(8,128)(2,1)S(1)} copy-done((bf16[2048,64]{0,1:T(8,128)(2,1)S(1)}, bf16[2048,64]{0,1:T(8,128)(2,1)}, u32[]{:S(2)}) %copy-start.6) | copy-done | bytes 262168
  9.0 0.9 %copy-done.7 = bf16[64,2048]{1,0:T(8,128)(2,1)S(1)} copy-done((bf16[64,2048]{1,0:T(8,128)(2,1)S(1)}, bf16[64,2048]{1,0:T(8,128)(2,1)}, u32[]{:S(2)}) %copy-start.7) | copy-done | bytes 262168
  9.9 0.8 %copy-done.8 = f32[256,64]{0,1:T(8,128)S(1)} copy-done((f32[256,64]{0,1:T(8,128)S(1)}, f32[256,64]{0,1:T(8,128)}, u32[]{:S(2)}) %copy-start.8) | copy-done | bytes 65560
  10.8 0.8 %copy-done.10 = bf16[256,64]{0,1:T(8,128)(2,1)S(1)} copy-done((bf16[256,64]{0,1:T(8,128)(2,1)S(1)}, bf16[256,64]{0,1:T(8,128)(2,1)}, u32[]{:S(2)}) %copy-start.10) | copy-done | bytes 32792
  11.5 0.8 %copy-done.11 = bf16[256,64]{0,1:T(8,128)(2,1)S(1)} copy-done((bf16[256,64]{0,1:T(8,128)(2,1)S(1)}, bf16[256,64]{0,1:T(8,128)(2,1)}, u32[]{:S(2)}) %copy-start.11) | copy-done | bytes 32792
  12.3 0.8 %copy-done.12 = bf16[256,64]{0,1:T(8,128)(2,1)S(1)} copy-done((bf16[256,64]{0,1:T(8,128)(2,1)S(1)}, bf16[256,64]{0,1:T(8,128)(2,1)}, u32[]{:S(2)}) %copy-start.12) | copy-done | bytes 32792
  13.0 0.8 %copy-done.13 = bf16[256,64]{0,1:T(8,128)(2,1)S(1)} copy-done((bf16[256,64]{0,1:T(8,128)(2,1)S(1)}, bf16[256,64]{0,1:T(8,128)(2,1)}, u32[]{:S(2)}) %copy-start.13) | copy-done | bytes 32792
  13.8 0.8 %copy-done.14 = bf16[256,64]{0,1:T(8,128)(2,1)S(1)} copy-done((bf16[256,64]{0,1:T(8,128)(2,1)S(1)}, bf16[256,64]{0,1:T(8,128)(2,1)}, u32[]{:S(2)}) %copy-start.14) | copy-done | bytes 32792
  14.6 0.7 copy-done.15
  15.3 0.7 copy-done.16
  16.0 0.7 copy-done.19
  16.6 0.7 copy-done.20
  17.3 54.5 %shard_map.212 = (bf16[16,2048]{1,0:T(8,128)(2,1)S(1)}, bf16[128,128]{1,0:T(8,128)(2,1)S(1)}) custom-call(bf16[64,256]{1,0:T(8,128)(2,1)S(1)} %bitcast.24, bf16[64,256]{1,0:T(8,128)(2,1)S(1)} %bitcast.25, bf16[64,256]{1,0:T(8,128)(2,1)S(1)} %bitcast.26, bf16[64,256]{1,0:T(8,128)(2,1)S(1)} %bitcast.27, bf16[64,256]{1,0:T(8,128)(2,1)S(1)} %bitcast.28, ...), custom_call_target="tpu_custom_call" | custom-call | tf_op jit(solution)/shard_map/pallas_call | solution.py:423
  71.8 0.6 copy.25
  72.4 0.6 copy.26
  (21 shorter events, 0.0 us)
Async XLA Ops:
  0.6 0.8 %copy-start.9 = (bf16[256,64]{0,1:T(8,128)(2,1)S(1)}, bf16[256,64]{0,1:T(8,128)(2,1)}, u32[]{:S(2)}) copy-start(bf16[256,64]{0,1:T(8,128)(2,1)} %param.21) | copy-start | bytes 98308
  0.6 0.8 %copy-start.18 = (f32[128,2]{0,1:T(2,128)S(1)}, f32[128,2]{0,1:T(2,128)}, u32[]{:S(2)}) copy-start(f32[128,2]{0,1:T(2,128)} %param.35) | copy-start | bytes 3076
  0.7 0.7 %copy-start.17 = (s32[128,2]{0,1:T(2,128)S(1)}, s32[128,2]{0,1:T(2,128)}, u32[]{:S(2)}) copy-start(s32[128,2]{0,1:T(2,128)} %param.34) | copy-start | bytes 3076
  1.4 1.2 %copy-start = (bf16[1,2048,256]{2,1,0:T(8,128)(2,1)S(1)}, bf16[1,2048,256]{2,1,0:T(8,128)(2,1)}, u32[]{:S(2)}) copy-start(bf16[1,2048,256]{2,1,0:T(8,128)(2,1)} %param.36) | copy-start | bytes 3145732
  2.6 1.2 %copy-start.1 = (bf16[1,2048,256]{2,1,0:T(8,128)(2,1)S(1)}, bf16[1,2048,256]{2,1,0:T(8,128)(2,1)}, u32[]{:S(2)}) copy-start(bf16[1,2048,256]{2,1,0:T(8,128)(2,1)} %param.37) | copy-start | bytes 3145732
  3.9 1.2 %copy-start.2 = (bf16[1,256,2048]{2,1,0:T(8,128)(2,1)S(1)}, bf16[1,256,2048]{2,1,0:T(8,128)(2,1)}, u32[]{:S(2)}) copy-start(bf16[1,256,2048]{2,1,0:T(8,128)(2,1)} %param.38) | copy-start | bytes 3145732
  5.1 1.0 %copy-start.3 = (bf16[128,2048]{1,0:T(8,128)(2,1)S(1)}, bf16[128,2048]{1,0:T(8,128)(2,1)}, u32[]{:S(2)}) copy-start(bf16[128,2048]{1,0:T(8,128)(2,1)} %refs_14_.1) | copy-start | bytes 1572868
  6.1 0.9 %copy-start.4 = (bf16[64,2048]{1,0:T(8,128)(2,1)S(1)}, bf16[64,2048]{1,0:T(8,128)(2,1)}, u32[]{:S(2)}) copy-start(bf16[64,2048]{1,0:T(8,128)(2,1)} %refs_13_.1) | copy-start | bytes 786436
  7.1 0.9 %copy-start.5 = (bf16[2048,64]{0,1:T(8,128)(2,1)S(1)}, bf16[2048,64]{0,1:T(8,128)(2,1)}, u32[]{:S(2)}) copy-start(bf16[2048,64]{0,1:T(8,128)(2,1)} %param.39) | copy-start | bytes 786436
  8.0 0.9 %copy-start.6 = (bf16[2048,64]{0,1:T(8,128)(2,1)S(1)}, bf16[2048,64]{0,1:T(8,128)(2,1)}, u32[]{:S(2)}) copy-start(bf16[2048,64]{0,1:T(8,128)(2,1)} %param.40) | copy-start | bytes 786436
  9.0 0.9 %copy-start.7 = (bf16[64,2048]{1,0:T(8,128)(2,1)S(1)}, bf16[64,2048]{1,0:T(8,128)(2,1)}, u32[]{:S(2)}) copy-start(bf16[64,2048]{1,0:T(8,128)(2,1)} %refs_20_.1) | copy-start | bytes 786436
  9.9 0.8 %copy-start.8 = (f32[256,64]{0,1:T(8,128)S(1)}, f32[256,64]{0,1:T(8,128)}, u32[]{:S(2)}) copy-start(f32[256,64]{0,1:T(8,128)} %param.28) | copy-start | bytes 196612
  10.8 0.8 %copy-start.10 = (bf16[256,64]{0,1:T(8,128)(2,1)S(1)}, bf16[256,64]{0,1:T(8,128)(2,1)}, u32[]{:S(2)}) copy-start(bf16[256,64]{0,1:T(8,128)(2,1)} %param.22) | copy-start | bytes 98308
  11.5 0.8 %copy-start.11 = (bf16[256,64]{0,1:T(8,128)(2,1)S(1)}, bf16[256,64]{0,1:T(8,128)(2,1)}, u32[]{:S(2)}) copy-start(bf16[256,64]{0,1:T(8,128)(2,1)} %param.23) | copy-start | bytes 98308
  12.3 0.8 %copy-start.12 = (bf16[256,64]{0,1:T(8,128)(2,1)S(1)}, bf16[256,64]{0,1:T(8,128)(2,1)}, u32[]{:S(2)}) copy-start(bf16[256,64]{0,1:T(8,128)(2,1)} %param.24) | copy-start | bytes 98308
  13.0 0.8 %copy-start.13 = (bf16[256,64]{0,1:T(8,128)(2,1)S(1)}, bf16[256,64]{0,1:T(8,128)(2,1)}, u32[]{:S(2)}) copy-start(bf16[256,64]{0,1:T(8,128)(2,1)} %param.25) | copy-start | bytes 98308
  13.8 0.8 %copy-start.14 = (bf16[256,64]{0,1:T(8,128)(2,1)S(1)}, bf16[256,64]{0,1:T(8,128)(2,1)}, u32[]{:S(2)}) copy-start(bf16[256,64]{0,1:T(8,128)(2,1)} %param.26) | copy-start | bytes 98308
  14.6 0.7 copy-start.15
  15.3 0.7 copy-start.16
  16.0 0.7 copy-start.19
  16.6 0.7 copy-start.20

commit v2 on v1

--- a/solution.py
+++ b/solution.py
@@ -12,6 +12,7 @@
 L = 128
 GROUPS = 8
 CAP = 2
+FAR_FIRST = (4, 3, 5, 2, 6, 1, 7)
 NORM_EPSILON = 1e-06
 GROUP_EPSILON = 0.00064
 F32 = jnp.float32
@@ -49,6 +50,21 @@
     return total
 
 
+def square(a, b):
+    (ah, al), (bh, bl) = parts(a, 2), parts(b, 2)
+    both = nn(
+        jnp.concatenate([ah, al], axis=1),
+        jnp.concatenate(
+            [
+                jnp.concatenate([bh, bl], axis=1),
+                jnp.concatenate([bh, jnp.zeros_like(bl)], axis=1),
+            ],
+            axis=0,
+        ),
+    )
+    return both[:, :L] + both[:, L:]
+
+
 def iota(shape, dim):
     return lax.broadcasted_iota(jnp.int32, shape, dim)
 
@@ -73,21 +89,25 @@
     return mm(late, beside_identity(early))
 
 
-def block_inverse(n):
+def solved(right, n):
     r, c = iota((L, L), 0), iota((L, L), 1)
     eye = jnp.where(r == c, 1.0, 0.0)
-    small = jnp.where(r // 8 == c // 8, n, 0.0)
-    two = mm(small, small)
-    four = mm(two, two)
-    first = eye + small + two + mm(small, two)
-    x = first + mm(first, four)
-    size = 8
-    while size < L:
-        lower, upper = r // size, c // size
-        off = jnp.where((upper == lower + 1) & (lax.rem(lower, 2) == 0), n, 0.0)
-        x = x + mm(mm(x, off), x)
-        size *= 2
-    return x
+    same8 = r // 8 == c // 8
+    same32 = r // 32 == c // 32
+    small = jnp.where(same8, n, 0.0)
+    middle = jnp.where(same32 & (r // 8 != c // 8), n, 0.0)
+    large = jnp.where(same32, 0.0, n)
+    two = square(small, small)
+    four = square(two, two)
+    first = eye + small + two + square(small, two)
+    x = first + square(first, four)
+    step = square(middle, x)
+    x = x + square(x, step)
+    x = x + square(x, square(step, step))
+    step = square(large, x)
+    y = square(right, x)
+    y = y + square(y, step)
+    return y + square(y, square(step, step))
 
 
 def local_block(rec, key, val, removal, lr, ld):
@@ -107,10 +127,14 @@
     ob = jnp.where(s <= t, both[:L, L:], 0.0)
     lk = jnp.where(s < t, both[L:, :L], 0.0)
     ok = jnp.where(s <= t, both[L:, L:], 0.0)
+    return lb, ob, lk, ok, kb, kk, qn, qr, eref, eend, jnp.exp(end), val
+
+
+def local_result(lb, ob, lk, ok, kb, kk, qn, qr, eref, eend, whole, val):
     valued = mm(val, jnp.concatenate([lk, ok], axis=1))
     right = jnp.concatenate([valued[:, :L], qn * eref], axis=0)
-    corr = mm(right, block_inverse(lb))
-    z = mm(corr, ob) + jnp.concatenate([valued[:, L:], qr * eref], axis=0)
+    corr = solved(right, lb)
+    z = square(corr, ob) + jnp.concatenate([valued[:, L:], qr * eref], axis=0)
     aug = jnp.concatenate([val, jnp.zeros_like(val)], axis=0)
     f = mm(
         jnp.concatenate([kb * eend, kk * eend], axis=1),
@@ -118,17 +142,16 @@
         nt,
     )
     f = f + jnp.where(
-        iota((HC, 2 * HC), 0) + HC == iota((HC, 2 * HC), 1), jnp.exp(end), 0.0
+        iota((HC, 2 * HC), 0) + HC == iota((HC, 2 * HC), 1), whole, 0.0
     )
     return f, z
 
 
 def kernel(nx, nz, *refs):
-    (rec, key, val, dec, lrn, gat, spk, dco, hng, png, eng, idx, wts) = refs[:13]
-    (how_h, exr_h, rg_h, ru_h, rd_h, cg_h, cu_h, cd_h) = refs[13:21]
+    from_hbm = refs[:21]
     out_a, out_b = refs[21:23]
-    (how, exr, rg, ru, rd, cgu, cd, nb, dout, darr, ep, epr, es, rb, rout, rarr,
-     sp, spr, ss, sb, ap, apr, aps, ab, xarr, zs, zarr, load, pair_s, pair_r, dsend, drecv,
+    (exr, eng, idx, cgu, cd, rec, key, val, dec, lrn, spk, dco, gat, hng, wts, rg, ru, rd, how, png, nb, dout, darr, ep, epr, es, rb, rout, rarr,
+     sp, spr, ss, sb, ho, ap, apr, aps, ab, xarr, zs, zarr, load, pair_s, pair_r, dsend, drecv,
      ysend, yrecv, rsend, rrecv, xsend, xrecv, zsend, zrecv) = refs[23:]
     n_ep = nx * nz
     tb = exr.shape[0]
@@ -148,15 +171,20 @@
     def drain(ref, sem):
         pltpu.make_async_copy(ref, ref, sem).wait()
 
+    targets = (
+        exr, eng, idx, cgu.at[0:HC], cgu.at[HC : 2 * HC], cd, rec, key, val, dec, lrn, spk, dco,
+        gat, hng, wts, rg, ru, rd, how, png,
+    )
     loads = [
         pltpu.make_async_copy(a, b, load.at[k])
-        for k, (a, b) in enumerate((
-            (exr_h, exr), (cg_h, cgu.at[0:HC]), (cu_h, cgu.at[HC : 2 * HC]), (cd_h, cd),
-            (rg_h, rg), (ru_h, ru), (rd_h, rd), (how_h, how),
-        ))
+        for k, (a, b) in enumerate(zip(from_hbm, targets, strict=True))
     ]
     for copy in loads:
         copy.start()
+
+    def ready(start, stop):
+        for copy in loads[start:stop]:
+            copy.wait()
 
     unit = jnp.where(iota((HC, 2 * HC), 0) + HC == iota((HC, 2 * HC), 1), 1.0, 0.0)
     for k in range(nz):
@@ -177,12 +205,12 @@
 
     lax.fori_loop(1, n_ep, greet, 0)
 
-    loads[0].wait()
+    ready(0, 3)
     wide = exr[...].astype(F32)
     scale = lax.rsqrt(jnp.mean(wide * wide, axis=1, keepdims=True) + NORM_EPSILON)
     nb[...] = (wide * scale * eng[...]).astype(BF16)
 
-    width = nb.shape[1] // GROUPS
+    width = darr.shape[2]
     first, second = idx[0:1, :], idx[1:2, :]
     i = iota((slots, tb), 0)
     expert = lax.div(i, 16) * GROUPS + y
@@ -195,15 +223,17 @@
         [jnp.where(piece == j, mine, 0.0).astype(BF16) for j in range(GROUPS)], axis=1
     )
     stacked = jnp.concatenate(
-        [nb[:, j * width : (j + 1) * width] for j in range(GROUPS)], axis=0
+        [
+            nb[:, pl.ds(pl.multiple_of((c * GROUPS + j) * width, width), width)]
+            for j in range(GROUPS)
+        ],
+        axis=0,
     )
     dout[...] = nn(picks, stacked).astype(BF16)
     own = pl.ds(pl.multiple_of(me * 16, 16), 16)
-    darr[own, :] = dout[own, :]
-
-    loads[1].wait()
-    loads[2].wait()
-    loads[3].wait()
+    darr[c, own, :] = dout[own, :]
+
+    ready(3, 6)
     gate_up = nt(cgu[...], nb[...])
     g, u = gate_up[:HC], gate_up[HC:]
     hidden = (g * sigmoid(g) * u).T.astype(BF16)
@@ -212,32 +242,35 @@
     for k in range(2 * GROUPS):
         sp[k % 2, k // 2] = shared[:, k * cols : (k + 1) * cols]
 
-    pl.semaphore_wait(barrier, GROUPS + n_ep - 1)
-
-    def send_rows(d, carry):
-        to = lax.rem(me + d, n_ep)
-        remote(
-            dout.at[pl.ds(pl.multiple_of(to * 16, 16), 16)], darr.at[own],
-            dsend, drecv, {"ep": to},
-        ).start()
-        return carry
-
-    lax.fori_loop(1, n_ep, send_rows, 0)
-    pair_shared = remote(sp.at[1 - c], spr, pair_s.at[0], pair_r.at[0], {"tp": other})
-    pair_shared.start()
-
+    ready(6, 13)
     k_in = key[...].astype(F32)
     pre = column(dco[...]) + jnp.tanh(dec[...].astype(F32))
     ld = spk[...] - sigmoid(pre) * math.exp(-0.5)
     lr = sigmoid(lrn[...].astype(F32))
     removal = k_in * lax.rsqrt(jnp.sum(k_in * k_in, axis=0, keepdims=True) + NORM_EPSILON)
     r_in = rec[...].astype(F32)
-    blocks = []
+    prepared = []
     for b in range(key.shape[1] // L):
         at = slice(b * L, (b + 1) * L)
-        blocks.append(
+        prepared.append(
             local_block(r_in[:, at], k_in[:, at], val[:, at], removal[:, at], lr[:, at], ld[:, at])
         )
+
+    pl.semaphore_wait(barrier, GROUPS + n_ep - 1)
+
+    def send_rows(d, carry):
+        to = lax.rem(me + d, n_ep)
+        remote(
+            dout.at[pl.ds(pl.multiple_of(to * 16, 16), 16)], darr.at[c, own],
+            dsend, drecv, {"ep": to},
+        ).start()
+        return carry
+
+    lax.fori_loop(1, n_ep, send_rows, 0)
+    pair_shared = remote(sp.at[1 - c], spr, pair_s.at[0], pair_r.at[0], {"tp": other})
+    pair_shared.start()
+
+    blocks = [local_result(*values) for values in prepared]
     f, z_out = blocks[0]
     z_all = [z_out]
     for later_f, later_z in blocks[1:]:
@@ -245,6 +278,7 @@
         f = joined(later_f, f)
     z_all = jnp.concatenate(z_all, axis=1)
     xarr[x] = f.astype(BF16)
+
     x_sends = [
         remote(
             xarr.at[x], xarr.at[x], xsend.at[d - 1], xrecv.at[d - 1],
@@ -259,30 +293,12 @@
     ss[...] = (sp[c].astype(F32) + spr[...].astype(F32)).astype(BF16)
     sb[y] = ss[y]
     y_sends = []
-    for d in range(1, GROUPS):
+    for k, d in enumerate(FAR_FIRST):
         to = lax.rem(y + d, GROUPS)
         y_sends.append(
-            remote(ss.at[to], sb.at[y], ysend.at[0, d - 1], yrecv.at[0, d - 1], {"tp": 2 * to + c})
+            remote(ss.at[to], sb.at[y], ysend.at[0, k], yrecv.at[0, k], {"tp": 2 * to + c})
         )
         y_sends[-1].start()
-
-    drain(darr.at[0 : (n_ep - 1) * 16], drecv)
-    r, q = iota((slots, slots), 0), iota((slots, slots), 1)
-    source = lax.rem(r, n_ep) * 16 + lax.rem(lax.div(r, n_ep), 2) * 8 + lax.div(r, rows)
-    turned = nn(jnp.where(q == source, 1.0, 0.0).astype(BF16), darr[...]).astype(BF16)
-    rows_in = jnp.concatenate(
-        [turned[j * rows : (j + 1) * rows] for j in range(GROUPS)], axis=1
-    )
-    loads[4].wait()
-    loads[5].wait()
-    g, u = nn(rows_in, rg[...]), nn(rows_in, ru[...])
-    hidden = (g * sigmoid(g) * u).astype(BF16)
-    loads[6].wait()
-    routed = nn(hidden, rd[...]).astype(BF16)
-    for k in range(2 * GROUPS):
-        ep[k % 2, k // 2] = routed[:, k * cols : (k + 1) * cols]
-    pair_routed = remote(ep.at[1 - c], epr, pair_s.at[1], pair_r.at[1], {"tp": other})
-    pair_routed.start()
 
     for copy in x_sends:
         copy.wait()
@@ -300,17 +316,9 @@
                 zs, zarr.at[z], zsend.at[d - 1], zrecv.at[z], {"ep": (z + d) * nx + x}
             ).start()
 
-    pair_routed.wait()
-    es[...] = (ep[c].astype(F32) + epr[...].astype(F32)).astype(BF16)
-    rb[y] = es[y]
-    for d in range(1, GROUPS):
-        to = lax.rem(y + d, GROUPS)
-        y_sends.append(
-            remote(es.at[to], rb.at[y], ysend.at[1, d - 1], yrecv.at[1, d - 1], {"tp": 2 * to + c})
-        )
-        y_sends[-1].start()
     z_all = mm(beside_identity(before).T, z_all)
 
+    ready(13, 16)
     q = iota((slots, slots), 1)
     r = iota((slots, slots), 0)
     source = lax.div(lax.rem(r, 16), 2) * rows + lax.rem(r, 2) * n_ep + lax.div(r, 16)
@@ -328,6 +336,98 @@
         rank == lax.rem(q, 2).astype(F32), hit_a * lines[:, 2:3] + hit_b * lines[:, 3:4], 0.0
     )
 
+    r, q = iota((slots, slots), 0), iota((slots, slots), 1)
+    source = lax.rem(r, n_ep) * 16 + lax.rem(lax.div(r, n_ep), 2) * 8 + lax.div(r, rows)
+    turn = jnp.where(q == source, 1.0, 0.0).astype(BF16)
+    drain(darr.at[c, 0 : (n_ep - 1) * 16], drecv)
+    pair_rows = remote(darr.at[c], darr.at[c], pair_s.at[4], pair_r.at[4], {"tp": other})
+    pair_rows.start()
+    pair_rows.wait()
+
+    turned = nn(turn, jnp.concatenate([darr[0], darr[1]], axis=1)).astype(BF16)
+    rows_in = jnp.concatenate(
+        [
+            turned[j * rows : (j + 1) * rows, h * width : (h + 1) * width]
+            for h in range(2)
+            for j in range(GROUPS)
+        ],
+        axis=1,
+    )
+    ready(16, 18)
+    g, u = nn(rows_in, rg[...]), nn(rows_in, ru[...])
+    hidden = (g * sigmoid(g) * u).astype(BF16)
+    ready(18, 19)
+    routed = nn(hidden, rd[...]).astype(BF16)
+    for k in range(2 * GROUPS):
+        ep[k % 2, k // 2] = routed[:, k * cols : (k + 1) * cols]
+    pair_routed = remote(ep.at[1 - c], epr, pair_s.at[1], pair_r.at[1], {"tp": other})
+    pair_routed.start()
+
+    pair_routed.wait()
+    es[...] = (ep[c].astype(F32) + epr[...].astype(F32)).astype(BF16)
+    rb[y] = es[y]
+    for k, d in enumerate(FAR_FIRST):
+        to = lax.rem(y + d, GROUPS)
+        y_sends.append(
+            remote(es.at[to], rb.at[y], ysend.at[1, k], yrecv.at[1, k], {"tp": 2 * to + c})
+        )
+        y_sends[-1].start()
+
+    for k in range(nz - 1):
+        @pl.when(k < z)
+        def _():
+            drain(zarr.at[k], zrecv.at[k])
+
+    level = [zarr[k] for k in range(nz - 1)] if nz > 1 else [unit.astype(BF16)]
+    while len(level) > 1:
+        nxt = [joined(level[k + 1], level[k]) for k in range(0, len(level) - 1, 2)]
+        if len(level) % 2:
+            nxt.append(level[-1].astype(F32))
+        level = nxt
+
+    carried = level[0].astype(F32)
+    head = mm(beside_identity(carried).T[:HC], z_all)
+    centred = head - jnp.mean(head, axis=0, keepdims=True)
+    normed = centred * lax.rsqrt(jnp.mean(centred * centred, axis=0, keepdims=True) + GROUP_EPSILON)
+    heads_out = normed * column(hng[...]) * sigmoid(gat[...].astype(F32))
+    heads_out = heads_out.T.astype(BF16)
+    own_rows = out_a.shape[0]
+    ho[...] = heads_out.reshape(GROUPS, 2, own_rows, HC)
+    ready(19, 20)
+
+    order = FAR_FIRST + (0,)
+    half = GROUPS // 2
+
+    def product(first, core):
+        lines = [ho[lax.rem(y + d, GROUPS), core] for d in order[first : first + half]]
+        return nn(jnp.concatenate(lines, axis=0), how[...])
+
+    pair_mix = []
+    for k in range(2):
+        at = slice(k * half, (k + 1) * half)
+        ap[at] = product(k * half, 1 - c).astype(BF16).reshape(half, own_rows, -1)
+        pair_mix.append(
+            remote(ap.at[at], apr.at[at], pair_s.at[2 + k], pair_r.at[2 + k], {"tp": other})
+        )
+        pair_mix[-1].start()
+    mixed = [product(k * half, c).astype(BF16).astype(F32) for k in range(2)]
+
+    a_sends = []
+    for k in range(2):
+        at = slice(k * half, (k + 1) * half)
+        pair_mix[k].wait()
+        aps[at] = (mixed[k].reshape(half, own_rows, -1) + apr[at].astype(F32)).astype(BF16)
+        for j in range(k * half, (k + 1) * half):
+            if order[j]:
+                to = lax.rem(y + order[j], GROUPS)
+                a_sends.append(
+                    remote(
+                        aps.at[j], ab.at[y], ysend.at[2, j], yrecv.at[2, j], {"tp": 2 * to + c}
+                    )
+                )
+                a_sends[-1].start()
+    ab[y] = aps[GROUPS - 1]
+
     for copy in y_sends[GROUPS - 1 :]:
         copy.wait()
     every = jnp.concatenate([rb[k] for k in range(GROUPS)], axis=0)
@@ -344,41 +444,6 @@
 
     lax.fori_loop(1, n_ep, send_back, 0)
 
-    for k in range(nz - 1):
-        @pl.when(k < z)
-        def _():
-            drain(zarr.at[k], zrecv.at[k])
-
-    level = [zarr[k] for k in range(nz - 1)] if nz > 1 else [unit.astype(BF16)]
-    while len(level) > 1:
-        nxt = [joined(level[k + 1], level[k]) for k in range(0, len(level) - 1, 2)]
-        if len(level) % 2:
-            nxt.append(level[-1].astype(F32))
-        level = nxt
-    carried = level[0].astype(F32)
-    head = mm(beside_identity(carried).T[:HC], z_all)
-    centred = head - jnp.mean(head, axis=0, keepdims=True)
-    normed = centred * lax.rsqrt(jnp.mean(centred * centred, axis=0, keepdims=True) + GROUP_EPSILON)
-    heads_out = normed * column(hng[...]) * sigmoid(gat[...].astype(F32))
-    heads_out = heads_out.T.astype(BF16)
-    loads[7].wait()
-    mixed = nn(heads_out, how[...]).astype(BF16)
-    own_rows = out_a.shape[0]
-    for k in range(2 * GROUPS):
-        ap[k % 2, k // 2] = mixed[k * own_rows : (k + 1) * own_rows]
-    pair_mix = remote(ap.at[1 - c], apr, pair_s.at[2], pair_r.at[2], {"tp": other})
-    pair_mix.start()
-    pair_mix.wait()
-    aps[...] = (ap[c].astype(F32) + apr[...].astype(F32)).astype(BF16)
-    ab[y] = aps[y]
-    a_sends = []
-    for d in range(1, GROUPS):
-        to = lax.rem(y + d, GROUPS)
-        a_sends.append(
-            remote(aps.at[to], ab.at[y], ysend.at[2, d - 1], yrecv.at[2, d - 1], {"tp": 2 * to + c})
-        )
-        a_sends[-1].start()
-
     for copy in y_sends[: GROUPS - 1]:
         copy.wait()
     drain(rarr.at[0 : (n_ep - 1) * 16], rrecv)
@@ -387,6 +452,7 @@
         answer = answer + sb[k].astype(F32)
     out_b[...] = answer.astype(BF16)
 
+    ready(20, 21)
     for copy in a_sends:
         copy.wait()
     mix = ab[0].astype(F32)
@@ -414,10 +480,14 @@
         tb = exr.shape[0]
         own, cols = ta // (2 * GROUPS), d // (2 * GROUPS)
         rows = n_ep * CAP
-        width = d // GROUPS
-        small = [a.T for a in (rec, key, val, dec, lrn, gat, spk)]
-        small += [a.reshape(1, -1) for a in (dco, hng, png, eng)] + [idx.T, wts.T]
-        large = [how, exr, rg[0], ru[0], rd[0], cg.T, cu.T, cd]
+        width = d // (2 * GROUPS)
+        line = lambda a: a.reshape(1, -1)
+        given = [
+            exr, line(eng), idx.T, cg.T, cu.T, cd, rec.T, key.T, val.T, dec.T, lrn.T, spk.T,
+            line(dco), gat.T, line(hng), wts.T, rg[0], ru[0], rd[0], how, line(png),
+        ]
+        held = [pltpu.VMEM(a.shape, a.dtype) for a in given]
+        held[3:5] = [pltpu.VMEM((2 * HC, d), BF16)]
         vmem = pl.BlockSpec(memory_space=pltpu.VMEM)
         dma = pltpu.SemaphoreType.DMA
         return pl.pallas_call(
@@ -426,19 +496,13 @@
                 jax.ShapeDtypeStruct((own, d), BF16),
                 jax.ShapeDtypeStruct((tb, cols), BF16),
             ),
-            in_specs=[vmem] * len(small) + [pl.BlockSpec(memory_space=pl.ANY)] * len(large),
+            in_specs=[pl.BlockSpec(memory_space=pltpu.HBM)] * len(given),
             out_specs=(vmem, vmem),
             scratch_shapes=[
-                pltpu.VMEM(how.shape, BF16),
-                pltpu.VMEM(exr.shape, BF16),
-                pltpu.VMEM(rg.shape[1:], BF16),
-                pltpu.VMEM(ru.shape[1:], BF16),
-                pltpu.VMEM(rd.shape[1:], BF16),
-                pltpu.VMEM((2 * HC, d), BF16),
-                pltpu.VMEM(cd.shape, BF16),
+                *held,
                 pltpu.VMEM((tb, d), BF16),
                 pltpu.VMEM((n_ep * 16, width), BF16),
-                pltpu.VMEM((n_ep * 16, width), BF16),
+                pltpu.VMEM((2, n_ep * 16, width), BF16),
                 pltpu.VMEM((2, GROUPS, rows, cols), BF16),
                 pltpu.VMEM((GROUPS, rows, cols), BF16),
                 pltpu.VMEM((GROUPS, rows, cols), BF16),
@@ -449,16 +513,17 @@
                 pltpu.VMEM((GROUPS, tb, cols), BF16),
                 pltpu.VMEM((GROUPS, tb, cols), BF16),
                 pltpu.VMEM((GROUPS, tb, cols), BF16),
-                pltpu.VMEM((2, GROUPS, own, d), BF16),
+                pltpu.VMEM((GROUPS, 2, own, HC), BF16),
+                pltpu.VMEM((GROUPS, own, d), BF16),
                 pltpu.VMEM((GROUPS, own, d), BF16),
                 pltpu.VMEM((GROUPS, own, d), BF16),
                 pltpu.VMEM((GROUPS, own, d), BF16),
                 pltpu.VMEM((nx, HC, 2 * HC), BF16),
                 pltpu.VMEM((HC, 2 * HC), BF16),
                 pltpu.VMEM((nz, HC, 2 * HC), BF16),
-                dma((8,)),
-                dma((3,)),
-                dma((3,)),
+                dma((len(given),)),
+                dma((5,)),
+                dma((5,)),
                 dma,
                 dma,
                 dma((3, GROUPS - 1)),
@@ -471,9 +536,9 @@
                 dma((max(nz, 1),)),
             ],
             compiler_params=pltpu.CompilerParams(
-                collective_id=0, has_side_effects=True, vmem_limit_bytes=48 * 1024 * 1024
+                collective_id=0, has_side_effects=True, vmem_limit_bytes=67_043_328
             ),
-        )(*small, *large)
+        )(*given)
 
     placed = (
         P("ep", "tp"), P("ep", "tp"), P("ep", "tp"), P("ep", "tp"), P("ep", "tp"), P("ep", "tp"),

time: 74 us -> 48.4 us (0.65); the launches traced: 73.1 us -> 48.2 us
  local copies, waits for them, and re-layouts: 17.8 us -> 2.1 us
  Pallas kernels: 54.5 us -> 45.5 us
    unnamed x44 -> x4, local copies, waits for them, and re-layouts: 17.8 us -> 2.1 us
    pallas_call x1, Pallas kernels: 54.5 us -> 45.5 us  [body(): pl.pallas_call(functools.partial(kernel, nx, nz), out_shape=(jax.ShapeDty...]
where the time goes in v2:
time: 48.4 us; the launch traced here: 48.2 us
  Pallas kernels  45.5 us (94%)
  local copies, waits for them, and re-layouts  2.1 us (4%)
  between operations  0.66 us (1%)
    pallas_call x1, Pallas kernels, body(): pl.pallas_call(functools.partial(kernel, nx, nz), out_shape=(jax.ShapeDty...  45.5 us
    unnamed x4, local copies, waits for them, and re-layouts  2.1 us

profile of v2, /device:TPU:1, one launch (start us, length us, event | category | flops | bytes accessed | tf_op | source)
XLA Modules:
  0.0 48.2 jit_solution(24129741489333448)
XLA Ops:
  0.6 45.5 %shard_map.212 = (bf16[16,2048]{1,0:T(8,128)(2,1)}, bf16[128,128]{1,0:T(8,128)(2,1)}) custom-call(bf16[128,2048]{1,0:T(8,128)(2,1)} %refs_0_.1, f32[1,2048]{1,0:T(1,128)} %bitcast.30, s32[2,128]{1,0:T(2,128)} %bitcast.32, bf16[64,2048]{1,0:T(8,128)(2,1)} %bitcast.21, bf16[64,2048]{1,0:T(8,128)(2,1)} %bitcast.22, bf16[64,2048]{1,0:T(8,128)(2,1)} %refs_5_.1, ...), custom_call_target="tpu_custom_call" | custom-call | tf_op jit(solution)/shard_map/pallas_call | solution.py:493
  46.1 0.0 copy-start
  46.1 1.5 %copy.25 = bf16[16,2048]{1,0:T(8,128)(2,1)} copy(bf16[16,2048]{1,0:T(8,128)(2,1)} %get-tuple-element.4) | data formatting | bytes 131072
  47.6 0.0 copy-done
  47.6 0.6 %copy.26 = bf16[128,128]{1,0:T(8,128)(2,1)} copy(bf16[128,128]{1,0:T(8,128)(2,1)S(1)} %copy-done) | data formatting | bytes 65536
Async XLA Ops:
  46.1 1.5 %copy-start = (bf16[128,128]{1,0:T(8,128)(2,1)S(1)}, bf16[128,128]{1,0:T(8,128)(2,1)}, u32[]{:S(2)}) copy-start(bf16[128,128]{1,0:T(8,128)(2,1)} %get-tuple-element.5) | copy-start | bytes 98308

commit v3 on v2

--- a/solution.py
+++ b/solution.py
@@ -151,8 +151,8 @@
     from_hbm = refs[:21]
     out_a, out_b = refs[21:23]
     (exr, eng, idx, cgu, cd, rec, key, val, dec, lrn, spk, dco, gat, hng, wts, rg, ru, rd, how, png, nb, dout, darr, ep, epr, es, rb, rout, rarr,
-     sp, spr, ss, sb, ho, ap, apr, aps, ab, xarr, zs, zarr, load, pair_s, pair_r, dsend, drecv,
-     ysend, yrecv, rsend, rrecv, xsend, xrecv, zsend, zrecv) = refs[23:]
+     sp, spr, ss, sb, ho, ap, apr, aps, ring_in, xarr, zs, zarr, load, pair_s, pair_r, dsend, drecv,
+     ysend, yrecv, rsum_s, rsum_r, rsend, rrecv, xsend, xrecv, zsend, zrecv, zsc) = refs[23:]
     n_ep = nx * nz
     tb = exr.shape[0]
     rows = n_ep * CAP
@@ -171,6 +171,10 @@
     def drain(ref, sem):
         pltpu.make_async_copy(ref, ref, sem).wait()
 
+    def ready(start, stop):
+        for copy in loads[start:stop]:
+            copy.wait()
+
     targets = (
         exr, eng, idx, cgu.at[0:HC], cgu.at[HC : 2 * HC], cd, rec, key, val, dec, lrn, spk, dco,
         gat, hng, wts, rg, ru, rd, how, png,
@@ -179,37 +183,31 @@
         pltpu.make_async_copy(a, b, load.at[k])
         for k, (a, b) in enumerate(zip(from_hbm, targets, strict=True))
     ]
-    for copy in loads:
+    for copy in loads[:3]:
         copy.start()
-
-    def ready(start, stop):
-        for copy in loads[start:stop]:
-            copy.wait()
 
     unit = jnp.where(iota((HC, 2 * HC), 0) + HC == iota((HC, 2 * HC), 1), 1.0, 0.0)
     for k in range(nz):
         zarr[k] = unit.astype(BF16)
 
     barrier = pltpu.get_barrier_semaphore()
-    pl.semaphore_signal(barrier, inc=1, device_id={"tp": other}, device_id_type=MESH)
-    for d in range(1, GROUPS):
-        pl.semaphore_signal(
-            barrier, inc=1, device_id={"tp": 2 * lax.rem(y + d, GROUPS) + c}, device_id_type=MESH
-        )
-
-    def greet(d, carry):
-        pl.semaphore_signal(
-            barrier, inc=1, device_id={"ep": lax.rem(me + d, n_ep)}, device_id_type=MESH
-        )
+
+    def greet(where):
+        pl.semaphore_signal(barrier, inc=1, device_id=where, device_id_type=MESH)
+
+    def greet_ep(d, carry):
+        greet({"ep": lax.rem(me + d, n_ep)})
         return carry
 
-    lax.fori_loop(1, n_ep, greet, 0)
-
-    ready(0, 3)
-    wide = exr[...].astype(F32)
-    scale = lax.rsqrt(jnp.mean(wide * wide, axis=1, keepdims=True) + NORM_EPSILON)
-    nb[...] = (wide * scale * eng[...]).astype(BF16)
-
+    lax.fori_loop(n_ep // 2, n_ep, greet_ep, 0)
+    lax.fori_loop(1, n_ep // 2, greet_ep, 0)
+    for d in FAR_FIRST:
+        greet({"tp": 2 * lax.rem(y + d, GROUPS) + c})
+    greet({"tp": other})
+
+    for k in (*range(6, 13), *range(3, 6), *range(16, 20), *range(13, 16), 20):
+        loads[k].start()
+    ready(2, 3)
     width = darr.shape[2]
     first, second = idx[0:1, :], idx[1:2, :]
     i = iota((slots, tb), 0)
@@ -222,6 +220,12 @@
     picks = jnp.concatenate(
         [jnp.where(piece == j, mine, 0.0).astype(BF16) for j in range(GROUPS)], axis=1
     )
+
+    ready(0, 2)
+    wide = exr[...].astype(F32)
+    scale = lax.rsqrt(jnp.mean(wide * wide, axis=1, keepdims=True) + NORM_EPSILON)
+    nb[...] = (wide * scale * eng[...]).astype(BF16)
+
     stacked = jnp.concatenate(
         [
             nb[:, pl.ds(pl.multiple_of((c * GROUPS + j) * width, width), width)]
@@ -233,14 +237,24 @@
     own = pl.ds(pl.multiple_of(me * 16, 16), 16)
     darr[c, own, :] = dout[own, :]
 
-    ready(3, 6)
-    gate_up = nt(cgu[...], nb[...])
-    g, u = gate_up[:HC], gate_up[HC:]
-    hidden = (g * sigmoid(g) * u).T.astype(BF16)
-    shared = nn(hidden, cd[...]).astype(BF16)
-    cols = shared.shape[1] // (2 * GROUPS)
-    for k in range(2 * GROUPS):
-        sp[k % 2, k // 2] = shared[:, k * cols : (k + 1) * cols]
+    def to_all(src, dst, send, recv, groups):
+        for zo in groups:
+            for xo in sorted(range(nx), key=lambda v: -min(v, nx - v)):
+                if zo or xo:
+                    to = lax.rem(z + zo, nz) * nx + lax.rem(x + xo, nx)
+                    remote(
+                        src.at[pl.ds(pl.multiple_of(to * 16, 16), 16)], dst, send, recv, {"ep": to}
+                    ).start()
+
+    far_z = sorted(range(1, nz), key=lambda v: -min(v, nz - v))
+
+    def meet():
+        pl.semaphore_wait(barrier, GROUPS + n_ep - 1)
+        to_all(dout, darr.at[c, own], dsend, drecv, (*far_z, 0))
+
+    @pl.when(z >= nz // 2)
+    def _():
+        meet()
 
     ready(6, 13)
     k_in = key[...].astype(F32)
@@ -256,19 +270,14 @@
             local_block(r_in[:, at], k_in[:, at], val[:, at], removal[:, at], lr[:, at], ld[:, at])
         )
 
-    pl.semaphore_wait(barrier, GROUPS + n_ep - 1)
-
-    def send_rows(d, carry):
-        to = lax.rem(me + d, n_ep)
-        remote(
-            dout.at[pl.ds(pl.multiple_of(to * 16, 16), 16)], darr.at[c, own],
-            dsend, drecv, {"ep": to},
-        ).start()
-        return carry
-
-    lax.fori_loop(1, n_ep, send_rows, 0)
-    pair_shared = remote(sp.at[1 - c], spr, pair_s.at[0], pair_r.at[0], {"tp": other})
-    pair_shared.start()
+    ready(3, 6)
+    gate_up = nt(cgu[...], nb[...])
+    g, u = gate_up[:HC], gate_up[HC:]
+    hidden = (g * sigmoid(g) * u).T.astype(BF16)
+    shared = nn(hidden, cd[...]).astype(BF16)
+    cols = shared.shape[1] // (2 * GROUPS)
+    for k in range(2 * GROUPS):
+        sp[k % 2, k // 2] = shared[:, k * cols : (k + 1) * cols]
 
     blocks = [local_result(*values) for values in prepared]
     f, z_out = blocks[0]
@@ -278,6 +287,10 @@
         f = joined(later_f, f)
     z_all = jnp.concatenate(z_all, axis=1)
     xarr[x] = f.astype(BF16)
+
+    @pl.when(z < nz // 2)
+    def _():
+        meet()
 
     x_sends = [
         remote(
@@ -289,34 +302,8 @@
     for copy in x_sends:
         copy.start()
 
-    pair_shared.wait()
-    ss[...] = (sp[c].astype(F32) + spr[...].astype(F32)).astype(BF16)
-    sb[y] = ss[y]
-    y_sends = []
-    for k, d in enumerate(FAR_FIRST):
-        to = lax.rem(y + d, GROUPS)
-        y_sends.append(
-            remote(ss.at[to], sb.at[y], ysend.at[0, k], yrecv.at[0, k], {"tp": 2 * to + c})
-        )
-        y_sends[-1].start()
-
-    for copy in x_sends:
-        copy.wait()
-    stretch = [xarr[k] for k in range(nx)]
-    before = unit
-    total = stretch[0]
-    for k in range(1, nx):
-        before = jnp.where(x == k, total.astype(F32), before)
-        total = joined(stretch[k], total)
-    zs[...] = total.astype(BF16)
-    for d in range(1, nz):
-        @pl.when(z + d < nz)
-        def _():
-            remote(
-                zs, zarr.at[z], zsend.at[d - 1], zrecv.at[z], {"ep": (z + d) * nx + x}
-            ).start()
-
-    z_all = mm(beside_identity(before).T, z_all)
+    pair_shared = remote(sp.at[1 - c], spr, pair_s.at[0], pair_r.at[0], {"tp": other})
+    pair_shared.start()
 
     ready(13, 16)
     q = iota((slots, slots), 1)
@@ -336,6 +323,103 @@
         rank == lax.rem(q, 2).astype(F32), hit_a * lines[:, 2:3] + hit_b * lines[:, 3:4], 0.0
     )
 
+    pair_shared.wait()
+    ss[...] = (sp[c].astype(F32) + spr[...].astype(F32)).astype(BF16)
+    sb[y] = ss[y]
+    y_sends = []
+    for k, d in enumerate(FAR_FIRST):
+        to = lax.rem(y + d, GROUPS)
+        y_sends.append(
+            remote(ss.at[to], sb.at[y], ysend.at[0, k], yrecv.at[0, k], {"tp": 2 * to + c})
+        )
+        y_sends[-1].start()
+
+    for copy in x_sends:
+        copy.wait()
+    stretch = [xarr[k] for k in range(nx)]
+    before = unit
+    total = stretch[0]
+    for k in range(1, nx):
+        before = jnp.where(x == k, total.astype(F32), before)
+        total = joined(stretch[k], total)
+    zs[...] = total.astype(BF16)
+    for d in range(1, nz):
+        @pl.when(z + d < nz)
+        def _():
+            remote(
+                zs, zarr.at[z], zsend.at[d - 1], zrecv.at[z], {"ep": (z + d) * nx + x}
+            ).start()
+
+    zsc[...] = mm(beside_identity(before).T, z_all)
+
+    order = FAR_FIRST + (0,)
+
+    def ring(step, way):
+        k = 3 * way + step
+        to = lax.rem(y + (GROUPS - 1 if way else 1), GROUPS)
+        slot = order.index(4 + step if way else 3 - step)
+        return remote(aps.at[slot], ring_in.at[k], rsum_s.at[k], rsum_r.at[k], {"tp": 2 * to + c})
+
+    def ring_on(step):
+        for way in range(2):
+            if step < 3 + way:
+                ring(step - 1, way).wait_recv()
+                slot = order.index(4 + step if way else 3 - step)
+                arrived = ring_in[3 * way + step - 1].astype(F32)
+                aps[slot] = (aps[slot].astype(F32) + arrived).astype(BF16)
+                ring(step, way).start()
+
+    def project_heads():
+        for k in range(nz - 1):
+            @pl.when(k < z)
+            def _():
+                drain(zarr.at[k], zrecv.at[k])
+
+        level = [zarr[k] for k in range(nz - 1)] if nz > 1 else [unit.astype(BF16)]
+        while len(level) > 1:
+            nxt = [joined(level[k + 1], level[k]) for k in range(0, len(level) - 1, 2)]
+            if len(level) % 2:
+                nxt.append(level[-1].astype(F32))
+            level = nxt
+
+        carried = level[0].astype(F32)
+        head = mm(beside_identity(carried).T[:HC], zsc[...])
+        centred = head - jnp.mean(head, axis=0, keepdims=True)
+        normed = centred * lax.rsqrt(jnp.mean(centred * centred, axis=0, keepdims=True) + GROUP_EPSILON)
+        heads_out = normed * column(hng[...]) * sigmoid(gat[...].astype(F32))
+        heads_out = heads_out.T.astype(BF16)
+        own_rows = out_a.shape[0]
+        ho[...] = heads_out.reshape(GROUPS, 2, own_rows, HC)
+        ready(19, 20)
+
+        half = GROUPS // 2
+
+        def product(first, core):
+            lines = [ho[lax.rem(y + d, GROUPS), core] for d in order[first : first + half]]
+            return nn(jnp.concatenate(lines, axis=0), how[...])
+
+        pair_mix = []
+        for k in range(2):
+            at = slice(k * half, (k + 1) * half)
+            ap[at] = product(k * half, 1 - c).astype(BF16).reshape(half, own_rows, -1)
+            pair_mix.append(
+                remote(ap.at[at], apr.at[at], pair_s.at[2 + k], pair_r.at[2 + k], {"tp": other})
+            )
+            pair_mix[-1].start()
+        mixed = [product(k * half, c).astype(BF16).astype(F32) for k in range(2)]
+
+        for k in range(2):
+            at = slice(k * half, (k + 1) * half)
+            pair_mix[k].wait()
+            aps[at] = (mixed[k].reshape(half, own_rows, -1) + apr[at].astype(F32)).astype(BF16)
+            if k == 0:
+                ring(0, 0).start()
+                ring(0, 1).start()
+
+    @pl.when(z < nz // 2)
+    def _():
+        project_heads()
+
     r, q = iota((slots, slots), 0), iota((slots, slots), 1)
     source = lax.rem(r, n_ep) * 16 + lax.rem(lax.div(r, n_ep), 2) * 8 + lax.div(r, rows)
     turn = jnp.where(q == source, 1.0, 0.0).astype(BF16)
@@ -373,60 +457,13 @@
         )
         y_sends[-1].start()
 
-    for k in range(nz - 1):
-        @pl.when(k < z)
-        def _():
-            drain(zarr.at[k], zrecv.at[k])
-
-    level = [zarr[k] for k in range(nz - 1)] if nz > 1 else [unit.astype(BF16)]
-    while len(level) > 1:
-        nxt = [joined(level[k + 1], level[k]) for k in range(0, len(level) - 1, 2)]
-        if len(level) % 2:
-            nxt.append(level[-1].astype(F32))
-        level = nxt
-
-    carried = level[0].astype(F32)
-    head = mm(beside_identity(carried).T[:HC], z_all)
-    centred = head - jnp.mean(head, axis=0, keepdims=True)
-    normed = centred * lax.rsqrt(jnp.mean(centred * centred, axis=0, keepdims=True) + GROUP_EPSILON)
-    heads_out = normed * column(hng[...]) * sigmoid(gat[...].astype(F32))
-    heads_out = heads_out.T.astype(BF16)
-    own_rows = out_a.shape[0]
-    ho[...] = heads_out.reshape(GROUPS, 2, own_rows, HC)
-    ready(19, 20)
-
-    order = FAR_FIRST + (0,)
-    half = GROUPS // 2
-
-    def product(first, core):
-        lines = [ho[lax.rem(y + d, GROUPS), core] for d in order[first : first + half]]
-        return nn(jnp.concatenate(lines, axis=0), how[...])
-
-    pair_mix = []
-    for k in range(2):
-        at = slice(k * half, (k + 1) * half)
-        ap[at] = product(k * half, 1 - c).astype(BF16).reshape(half, own_rows, -1)
-        pair_mix.append(
-            remote(ap.at[at], apr.at[at], pair_s.at[2 + k], pair_r.at[2 + k], {"tp": other})
-        )
-        pair_mix[-1].start()
-    mixed = [product(k * half, c).astype(BF16).astype(F32) for k in range(2)]
-
-    a_sends = []
-    for k in range(2):
-        at = slice(k * half, (k + 1) * half)
-        pair_mix[k].wait()
-        aps[at] = (mixed[k].reshape(half, own_rows, -1) + apr[at].astype(F32)).astype(BF16)
-        for j in range(k * half, (k + 1) * half):
-            if order[j]:
-                to = lax.rem(y + order[j], GROUPS)
-                a_sends.append(
-                    remote(
-                        aps.at[j], ab.at[y], ysend.at[2, j], yrecv.at[2, j], {"tp": 2 * to + c}
-                    )
-                )
-                a_sends[-1].start()
-    ab[y] = aps[GROUPS - 1]
+    @pl.when(z >= nz // 2)
+    def _():
+        project_heads()
+
+    @pl.when(z < nz // 2)
+    def _():
+        ring_on(1)
 
     for copy in y_sends[GROUPS - 1 :]:
         copy.wait()
@@ -434,15 +471,21 @@
     rout[...] = nn(back, every).astype(BF16)
     rarr[own, :] = rout[own, :]
 
-    def send_back(d, carry):
-        to = lax.rem(me + d, n_ep)
-        remote(
-            rout.at[pl.ds(pl.multiple_of(to * 16, 16), 16)], rarr.at[own],
-            rsend, rrecv, {"ep": to},
-        ).start()
-        return carry
-
-    lax.fori_loop(1, n_ep, send_back, 0)
+    to_all(rout, rarr.at[own], rsend, rrecv, (*far_z, 0))
+
+    @pl.when(z >= nz // 2)
+    def _():
+        ring_on(1)
+
+    ring_on(2)
+    ring_on(3)
+
+    ready(20, 21)
+    ring(2, 0).wait_recv()
+    ring(3, 1).wait_recv()
+    mix = aps[GROUPS - 1].astype(F32) + ring_in[2].astype(F32) + ring_in[6].astype(F32)
+    scale = lax.rsqrt(jnp.mean(mix * mix, axis=1, keepdims=True) + NORM_EPSILON)
+    out_a[...] = (mix * scale * png[...]).astype(BF16)
 
     for copy in y_sends[: GROUPS - 1]:
         copy.wait()
@@ -452,19 +495,14 @@
         answer = answer + sb[k].astype(F32)
     out_b[...] = answer.astype(BF16)
 
-    ready(20, 21)
-    for copy in a_sends:
-        copy.wait()
-    mix = ab[0].astype(F32)
-    for k in range(1, GROUPS):
-        mix = mix + ab[k].astype(F32)
-    scale = lax.rsqrt(jnp.mean(mix * mix, axis=1, keepdims=True) + NORM_EPSILON)
-    out_a[...] = (mix * scale * png[...]).astype(BF16)
 
     for d in range(1, nz):
         @pl.when(z + d < nz)
         def _():
             drain(zs, zsend.at[d - 1])
+    for way in range(2):
+        for step in range(3 + way):
+            ring(step, way).wait_send()
     drain(dout.at[0 : (n_ep - 1) * 16], dsend)
     drain(rout.at[0 : (n_ep - 1) * 16], rsend)
 
@@ -488,7 +526,9 @@
         ]
         held = [pltpu.VMEM(a.shape, a.dtype) for a in given]
         held[3:5] = [pltpu.VMEM((2 * HC, d), BF16)]
+        hbm = pl.BlockSpec(memory_space=pltpu.HBM)
         vmem = pl.BlockSpec(memory_space=pltpu.VMEM)
+        given = [pltpu.with_memory_space_constraint(a, pltpu.HBM) for a in given]
         dma = pltpu.SemaphoreType.DMA
         return pl.pallas_call(
             functools.partial(kernel, nx, nz),
@@ -496,7 +536,7 @@
                 jax.ShapeDtypeStruct((own, d), BF16),
                 jax.ShapeDtypeStruct((tb, cols), BF16),
             ),
-            in_specs=[pl.BlockSpec(memory_space=pltpu.HBM)] * len(given),
+            in_specs=[hbm] * len(given),
             out_specs=(vmem, vmem),
             scratch_shapes=[
                 *held,
@@ -517,7 +557,7 @@
                 pltpu.VMEM((GROUPS, own, d), BF16),
                 pltpu.VMEM((GROUPS, own, d), BF16),
                 pltpu.VMEM((GROUPS, own, d), BF16),
-                pltpu.VMEM((GROUPS, own, d), BF16),
+                pltpu.VMEM((GROUPS - 1, own, d), BF16),
                 pltpu.VMEM((nx, HC, 2 * HC), BF16),
                 pltpu.VMEM((HC, 2 * HC), BF16),
                 pltpu.VMEM((nz, HC, 2 * HC), BF16),
@@ -526,17 +566,20 @@
                 dma((5,)),
                 dma,
                 dma,
-                dma((3, GROUPS - 1)),
-                dma((3, GROUPS - 1)),
+                dma((2, GROUPS - 1)),
+                dma((2, GROUPS - 1)),
+                dma((7,)),
+                dma((7,)),
                 dma,
                 dma,
                 dma((max(nx - 1, 1),)),
                 dma((max(nx - 1, 1),)),
                 dma((max(nz - 1, 1),)),
                 dma((max(nz, 1),)),
+                pltpu.VMEM((2 * HC, ta), F32),
             ],
             compiler_params=pltpu.CompilerParams(
-                collective_id=0, has_side_effects=True, vmem_limit_bytes=67_043_328
+                collective_id=0, has_side_effects=True, vmem_limit_bytes=48 * 1024 * 1024
             ),
         )(*given)
 

time: 48.4 us -> 44.7 us (0.924)
  Pallas kernels: 45.5 us -> 42.3 us
  local copies, waits for them, and re-layouts: 2.1 us -> 1.25 us
    pallas_call x1, Pallas kernels: 45.5 us -> 42.3 us  [body(): pl.pallas_call(functools.partial(kernel, nx, nz), out_shape=(jax.ShapeDty...]
    unnamed x4 -> x2, local copies, waits for them, and re-layouts: 2.1 us -> 1.25 us
where the time goes in v3:
time: 44.7 us; the launch traced here: 44.2 us
  Pallas kernels  42.3 us (95%)
  local copies, waits for them, and re-layouts  1.25 us (3%)
  between operations  0.65 us (1%)
    pallas_call x1, Pallas kernels, body(): pl.pallas_call(functools.partial(kernel, nx, nz), out_shape=(jax.ShapeDty...  42.3 us
    unnamed x2, local copies, waits for them, and re-layouts  1.25 us

profile of v3, /device:TPU:1, one launch (start us, length us, event | category | flops | bytes accessed | tf_op | source)
XLA Modules:
  0.0 44.2 jit_solution(8485162855342044842)
XLA Ops:
  0.6 42.3 %shard_map.212 = (bf16[16,2048]{1,0:T(8,128)(2,1)S(1)}, bf16[128,128]{1,0:T(8,128)(2,1)S(1)}) custom-call(bf16[128,2048]{1,0:T(8,128)(2,1)} %refs_0_.1, f32[1,2048]{1,0:T(1,128)} %bitcast.30, s32[2,128]{1,0:T(2,128)} %bitcast.32, bf16[64,2048]{1,0:T(8,128)(2,1)} %bitcast.21, bf16[64,2048]{1,0:T(8,128)(2,1)} %bitcast.22, bf16[64,2048]{1,0:T(8,128)(2,1)} %refs_5_.1, ...), custom_call_target="tpu_custom_call" | custom-call | tf_op jit(solution)/shard_map/pallas_call | solution.py:533
  43.0 0.6 %copy.25 = bf16[16,2048]{1,0:T(8,128)(2,1)} copy(bf16[16,2048]{1,0:T(8,128)(2,1)S(1)} %get-tuple-element.4) | data formatting | bytes 131072
  43.6 0.6 %copy.26 = bf16[128,128]{1,0:T(8,128)(2,1)} copy(bf16[128,128]{1,0:T(8,128)(2,1)S(1)} %get-tuple-element.5) | data formatting | bytes 65536

commit v4 on v3

--- a/solution.py
+++ b/solution.py
@@ -150,9 +150,9 @@
 def kernel(nx, nz, *refs):
     from_hbm = refs[:21]
     out_a, out_b = refs[21:23]
-    (exr, eng, idx, cgu, cd, rec, key, val, dec, lrn, spk, dco, gat, hng, wts, rg, ru, rd, how, png, nb, dout, darr, ep, epr, es, rb, rout, rarr,
+    (exr, eng, idx, cgu, cd, rec, key, val, dec, lrn, spk, dco, gat, hng, wts, rg, ru, rd, how, png, nb, dout, darr, ep, epr, es, rarr,
      sp, spr, ss, sb, ho, ap, apr, aps, ring_in, xarr, zs, zarr, load, pair_s, pair_r, dsend, drecv,
-     ysend, yrecv, rsum_s, rsum_r, rsend, rrecv, xsend, xrecv, zsend, zrecv, zsc) = refs[23:]
+     seen, ysend, yrecv, rsum_s, rsum_r, rsend, rrecv, xsend, xrecv, zsend, zrecv, zsc) = refs[23:]
     n_ep = nx * nz
     tb = exr.shape[0]
     rows = n_ep * CAP
@@ -192,65 +192,56 @@
 
     barrier = pltpu.get_barrier_semaphore()
 
-    def greet(where):
-        pl.semaphore_signal(barrier, inc=1, device_id=where, device_id_type=MESH)
+    def greet(semaphore, where):
+        pl.semaphore_signal(semaphore, inc=1, device_id=where, device_id_type=MESH)
 
     def greet_ep(d, carry):
-        greet({"ep": lax.rem(me + d, n_ep)})
+        greet(barrier, {"ep": lax.rem(me + d, n_ep)})
         return carry
 
     lax.fori_loop(n_ep // 2, n_ep, greet_ep, 0)
     lax.fori_loop(1, n_ep // 2, greet_ep, 0)
     for d in FAR_FIRST:
-        greet({"tp": 2 * lax.rem(y + d, GROUPS) + c})
-    greet({"tp": other})
+        greet(barrier, {"tp": 2 * lax.rem(y + d, GROUPS) + c})
+    greet(barrier, {"tp": other})
 
     for k in (*range(6, 13), *range(3, 6), *range(16, 20), *range(13, 16), 20):
         loads[k].start()
     ready(2, 3)
-    width = darr.shape[2]
     first, second = idx[0:1, :], idx[1:2, :]
-    i = iota((slots, tb), 0)
-    expert = lax.div(i, 16) * GROUPS + y
+    i = iota((rows, tb), 0)
+    expert = lax.div(i, CAP) * GROUPS + y
     hits = jnp.where((first == expert) | (second == expert), 1.0, 0.0)
     earlier = jnp.where(iota((tb, tb), 0) < iota((tb, tb), 1), 1.0, 0.0).astype(BF16)
     rank = nn(hits.astype(BF16), earlier)
-    mine = jnp.where(rank == lax.rem(lax.div(i, 8), 2).astype(F32), hits, 0.0)
-    piece = lax.rem(i, 8)
-    picks = jnp.concatenate(
-        [jnp.where(piece == j, mine, 0.0).astype(BF16) for j in range(GROUPS)], axis=1
-    )
+    picks = jnp.where(rank == lax.rem(i, CAP).astype(F32), hits, 0.0).astype(BF16)
 
     ready(0, 2)
     wide = exr[...].astype(F32)
     scale = lax.rsqrt(jnp.mean(wide * wide, axis=1, keepdims=True) + NORM_EPSILON)
     nb[...] = (wide * scale * eng[...]).astype(BF16)
 
-    stacked = jnp.concatenate(
-        [
-            nb[:, pl.ds(pl.multiple_of((c * GROUPS + j) * width, width), width)]
-            for j in range(GROUPS)
-        ],
-        axis=0,
-    )
-    dout[...] = nn(picks, stacked).astype(BF16)
-    own = pl.ds(pl.multiple_of(me * 16, 16), 16)
-    darr[c, own, :] = dout[own, :]
-
-    def to_all(src, dst, send, recv, groups):
-        for zo in groups:
-            for xo in sorted(range(nx), key=lambda v: -min(v, nx - v)):
-                if zo or xo:
-                    to = lax.rem(z + zo, nz) * nx + lax.rem(x + xo, nx)
-                    remote(
-                        src.at[pl.ds(pl.multiple_of(to * 16, 16), 16)], dst, send, recv, {"ep": to}
-                    ).start()
+    width = dout.shape[2]
+    mine = nb[:, pl.ds(pl.multiple_of(c * width, width), width)]
+    dout[...] = nn(picks, mine).reshape(n_ep, CAP, width).astype(BF16)
+    darr[c, me] = dout[me]
+
+    def offsets():
+        return [(zo, xo) for zo in (*far_z, 0) for xo in far_x]
 
     far_z = sorted(range(1, nz), key=lambda v: -min(v, nz - v))
+    far_x = sorted(range(nx), key=lambda v: -min(v, nx - v))
+
+    pair_shared = remote(sp.at[1 - c], spr, pair_s.at[0], pair_r.at[0], {"tp": other})
 
     def meet():
         pl.semaphore_wait(barrier, GROUPS + n_ep - 1)
-        to_all(dout, darr.at[c, own], dsend, drecv, (*far_z, 0))
+        for d in FAR_FIRST:
+            greet(seen, {"tp": 2 * lax.rem(y + d, GROUPS) + c})
+        for zo, xo in offsets():
+            if zo or xo:
+                to = lax.rem(z + zo, nz) * nx + lax.rem(x + xo, nx)
+                remote(dout.at[to], darr.at[c, me], dsend, drecv, {"ep": to}).start()
 
     @pl.when(z >= nz // 2)
     def _():
@@ -279,6 +270,10 @@
     for k in range(2 * GROUPS):
         sp[k % 2, k // 2] = shared[:, k * cols : (k + 1) * cols]
 
+    @pl.when(z >= nz // 2)
+    def _():
+        pair_shared.start()
+
     blocks = [local_result(*values) for values in prepared]
     f, z_out = blocks[0]
     z_all = [z_out]
@@ -291,6 +286,7 @@
     @pl.when(z < nz // 2)
     def _():
         meet()
+        pair_shared.start()
 
     x_sends = [
         remote(
@@ -302,14 +298,7 @@
     for copy in x_sends:
         copy.start()
 
-    pair_shared = remote(sp.at[1 - c], spr, pair_s.at[0], pair_r.at[0], {"tp": other})
-    pair_shared.start()
-
     ready(13, 16)
-    q = iota((slots, slots), 1)
-    r = iota((slots, slots), 0)
-    source = lax.div(lax.rem(r, 16), 2) * rows + lax.rem(r, 2) * n_ep + lax.div(r, 16)
-    back = jnp.where(q == source, 1.0, 0.0).astype(BF16)
     lines = jnp.concatenate(
         [first.astype(F32), second.astype(F32), wts[...], jnp.zeros((4, tb), F32)], axis=0
     ).T
@@ -330,7 +319,7 @@
     for k, d in enumerate(FAR_FIRST):
         to = lax.rem(y + d, GROUPS)
         y_sends.append(
-            remote(ss.at[to], sb.at[y], ysend.at[0, k], yrecv.at[0, k], {"tp": 2 * to + c})
+            remote(ss.at[to], sb.at[y], ysend.at[k], yrecv.at[k], {"tp": 2 * to + c})
         )
         y_sends[-1].start()
 
@@ -420,23 +409,12 @@
     def _():
         project_heads()
 
-    r, q = iota((slots, slots), 0), iota((slots, slots), 1)
-    source = lax.rem(r, n_ep) * 16 + lax.rem(lax.div(r, n_ep), 2) * 8 + lax.div(r, rows)
-    turn = jnp.where(q == source, 1.0, 0.0).astype(BF16)
-    drain(darr.at[c, 0 : (n_ep - 1) * 16], drecv)
+    drain(darr.at[c, 0 : n_ep - 1], drecv)
     pair_rows = remote(darr.at[c], darr.at[c], pair_s.at[4], pair_r.at[4], {"tp": other})
     pair_rows.start()
     pair_rows.wait()
 
-    turned = nn(turn, jnp.concatenate([darr[0], darr[1]], axis=1)).astype(BF16)
-    rows_in = jnp.concatenate(
-        [
-            turned[j * rows : (j + 1) * rows, h * width : (h + 1) * width]
-            for h in range(2)
-            for j in range(GROUPS)
-        ],
-        axis=1,
-    )
+    rows_in = jnp.concatenate([darr[h].reshape(rows, width) for h in range(2)], axis=1)
     ready(16, 18)
     g, u = nn(rows_in, rg[...]), nn(rows_in, ru[...])
     hidden = (g * sigmoid(g) * u).astype(BF16)
@@ -448,35 +426,32 @@
     pair_routed.start()
 
     pair_routed.wait()
-    es[...] = (ep[c].astype(F32) + epr[...].astype(F32)).astype(BF16)
-    rb[y] = es[y]
-    for k, d in enumerate(FAR_FIRST):
-        to = lax.rem(y + d, GROUPS)
-        y_sends.append(
-            remote(es.at[to], rb.at[y], ysend.at[1, k], yrecv.at[1, k], {"tp": 2 * to + c})
-        )
-        y_sends[-1].start()
+    both = ep[c].astype(F32) + epr[...].astype(F32)
+    es[...] = both.reshape(GROUPS * n_ep, CAP, cols).astype(BF16)
+    place = me * GROUPS + y
+    rarr[place] = es[y * n_ep + me]
+    pl.semaphore_wait(seen, GROUPS - 1)
+
+    def send_back(k, carry):
+        yo = lax.rem(y + GROUPS // 2 + k, GROUPS)
+        for zo, xo in offsets():
+            to = lax.rem(z + zo, nz) * nx + lax.rem(x + xo, nx)
+            copy = remote(
+                es.at[yo * n_ep + to], rarr.at[place], rsend, rrecv, {"ep": to, "tp": 2 * yo + c}
+            )
+            if zo or xo:
+                copy.start()
+            else:
+                pl.when(yo != y)(copy.start)
+        return carry
+
+    lax.fori_loop(0, GROUPS, send_back, 0)
 
     @pl.when(z >= nz // 2)
     def _():
         project_heads()
 
-    @pl.when(z < nz // 2)
-    def _():
-        ring_on(1)
-
-    for copy in y_sends[GROUPS - 1 :]:
-        copy.wait()
-    every = jnp.concatenate([rb[k] for k in range(GROUPS)], axis=0)
-    rout[...] = nn(back, every).astype(BF16)
-    rarr[own, :] = rout[own, :]
-
-    to_all(rout, rarr.at[own], rsend, rrecv, (*far_z, 0))
-
-    @pl.when(z >= nz // 2)
-    def _():
-        ring_on(1)
-
+    ring_on(1)
     ring_on(2)
     ring_on(3)
 
@@ -487,10 +462,10 @@
     scale = lax.rsqrt(jnp.mean(mix * mix, axis=1, keepdims=True) + NORM_EPSILON)
     out_a[...] = (mix * scale * png[...]).astype(BF16)
 
-    for copy in y_sends[: GROUPS - 1]:
+    for copy in y_sends:
         copy.wait()
-    drain(rarr.at[0 : (n_ep - 1) * 16], rrecv)
-    answer = mm(weight, rarr[...])
+    drain(rarr.at[0 : n_ep * GROUPS - 1], rrecv)
+    answer = mm(weight, rarr[...].reshape(slots, cols))
     for k in range(GROUPS):
         answer = answer + sb[k].astype(F32)
     out_b[...] = answer.astype(BF16)
@@ -503,8 +478,8 @@
     for way in range(2):
         for step in range(3 + way):
             ring(step, way).wait_send()
-    drain(dout.at[0 : (n_ep - 1) * 16], dsend)
-    drain(rout.at[0 : (n_ep - 1) * 16], rsend)
+    drain(dout.at[0 : n_ep - 1], dsend)
+    drain(es.at[0 : n_ep * GROUPS - 1], rsend)
 
 
 def solution(mesh):
@@ -518,7 +493,6 @@
         tb = exr.shape[0]
         own, cols = ta // (2 * GROUPS), d // (2 * GROUPS)
         rows = n_ep * CAP
-        width = d // (2 * GROUPS)
         line = lambda a: a.reshape(1, -1)
         given = [
             exr, line(eng), idx.T, cg.T, cu.T, cd, rec.T, key.T, val.T, dec.T, lrn.T, spk.T,
@@ -541,14 +515,12 @@
             scratch_shapes=[
                 *held,
                 pltpu.VMEM((tb, d), BF16),
-                pltpu.VMEM((n_ep * 16, width), BF16),
-                pltpu.VMEM((2, n_ep * 16, width), BF16),
+                pltpu.VMEM((n_ep, CAP, d // 2), BF16),
+                pltpu.VMEM((2, n_ep, CAP, d // 2), BF16),
                 pltpu.VMEM((2, GROUPS, rows, cols), BF16),
                 pltpu.VMEM((GROUPS, rows, cols), BF16),
-                pltpu.VMEM((GROUPS, rows, cols), BF16),
-                pltpu.VMEM((GROUPS, rows, cols), BF16),
-                pltpu.VMEM((n_ep * 16, cols), BF16),
-                pltpu.VMEM((n_ep * 16, cols), BF16),
+                pltpu.VMEM((GROUPS * n_ep, CAP, cols), BF16),
+                pltpu.VMEM((GROUPS * n_ep, CAP, cols), BF16),
                 pltpu.VMEM((2, GROUPS, tb, cols), BF16),
                 pltpu.VMEM((GROUPS, tb, cols), BF16),
                 pltpu.VMEM((GROUPS, tb, cols), BF16),
@@ -566,8 +538,9 @@
                 dma((5,)),
                 dma,
                 dma,
-                dma((2, GROUPS - 1)),
-                dma((2, GROUPS - 1)),
+                pltpu.SemaphoreType.REGULAR,
+                dma((GROUPS - 1,)),
+                dma((GROUPS - 1,)),
                 dma((7,)),
                 dma((7,)),
                 dma,

time: 44.7 us -> 43.3 us (0.969)
  the two profiles are of different devices: /device:TPU:1 before, /device:TPU:256 now
where the time goes in v4:
time: 43.3 us; the launch traced here: 43.2 us
  Pallas kernels  41.3 us (95%)
  local copies, waits for them, and re-layouts  1.25 us (3%)
  between operations  0.65 us (2%)
    pallas_call x1, Pallas kernels, body(): pl.pallas_call(functools.partial(kernel, nx, nz), out_shape=(jax.ShapeDty...  41.3 us
    unnamed x2, local copies, waits for them, and re-layouts  1.25 us

profile of v4, /device:TPU:256, one launch (start us, length us, event | category | flops | bytes accessed | tf_op | source)
XLA Modules:
  0.0 43.2 jit_solution(2133782721066333238)
XLA Ops:
  0.6 41.3 %shard_map.212 = (bf16[16,2048]{1,0:T(8,128)(2,1)S(1)}, bf16[128,128]{1,0:T(8,128)(2,1)S(1)}) custom-call(bf16[128,2048]{1,0:T(8,128)(2,1)} %refs_0_.1, f32[1,2048]{1,0:T(1,128)} %bitcast.30, s32[2,128]{1,0:T(2,128)} %bitcast.32, bf16[64,2048]{1,0:T(8,128)(2,1)} %bitcast.21, bf16[64,2048]{1,0:T(8,128)(2,1)} %bitcast.22, bf16[64,2048]{1,0:T(8,128)(2,1)} %refs_5_.1, ...), custom_call_target="tpu_custom_call" | custom-call | tf_op jit(solution)/shard_map/pallas_call | solution.py:507
  41.9 0.6 %copy.25 = bf16[16,2048]{1,0:T(8,128)(2,1)} copy(bf16[16,2048]{1,0:T(8,128)(2,1)S(1)} %get-tuple-element.4) | data formatting | bytes 131072
  42.6 0.6 %copy.26 = bf16[128,128]{1,0:T(8,128)(2,1)} copy(bf16[128,128]{1,0:T(8,128)(2,1)S(1)} %get-tuple-element.5) | data formatting | bytes 65536

commit v5 on v4

--- a/solution.py
+++ b/solution.py
@@ -208,10 +208,10 @@
     for k in (*range(6, 13), *range(3, 6), *range(16, 20), *range(13, 16), 20):
         loads[k].start()
     ready(2, 3)
-    first, second = idx[0:1, :], idx[1:2, :]
+    choice_a, choice_b = idx[0:1, :], idx[1:2, :]
     i = iota((rows, tb), 0)
     expert = lax.div(i, CAP) * GROUPS + y
-    hits = jnp.where((first == expert) | (second == expert), 1.0, 0.0)
+    hits = jnp.where((choice_a == expert) | (choice_b == expert), 1.0, 0.0)
     earlier = jnp.where(iota((tb, tb), 0) < iota((tb, tb), 1), 1.0, 0.0).astype(BF16)
     rank = nn(hits.astype(BF16), earlier)
     picks = jnp.where(rank == lax.rem(i, CAP).astype(F32), hits, 0.0).astype(BF16)
@@ -243,7 +243,10 @@
                 to = lax.rem(z + zo, nz) * nx + lax.rem(x + xo, nx)
                 remote(dout.at[to], darr.at[c, me], dsend, drecv, {"ep": to}).start()
 
-    @pl.when(z >= nz // 2)
+    last = (z >= nz // 2) & (y >= GROUPS // 2)
+    first = (z < nz // 2) | (y == 0)
+
+    @pl.when(last)
     def _():
         meet()
 
@@ -270,7 +273,11 @@
     for k in range(2 * GROUPS):
         sp[k % 2, k // 2] = shared[:, k * cols : (k + 1) * cols]
 
-    @pl.when(z >= nz // 2)
+    @pl.when(jnp.logical_not(last | first))
+    def _():
+        meet()
+
+    @pl.when(jnp.logical_not(first))
     def _():
         pair_shared.start()
 
@@ -283,7 +290,7 @@
     z_all = jnp.concatenate(z_all, axis=1)
     xarr[x] = f.astype(BF16)
 
-    @pl.when(z < nz // 2)
+    @pl.when(first)
     def _():
         meet()
         pair_shared.start()
@@ -300,7 +307,7 @@
 
     ready(13, 16)
     lines = jnp.concatenate(
-        [first.astype(F32), second.astype(F32), wts[...], jnp.zeros((4, tb), F32)], axis=0
+        [choice_a.astype(F32), choice_b.astype(F32), wts[...], jnp.zeros((4, tb), F32)], axis=0
     ).T
     q = iota((tb, slots), 1)
     expert = (lax.div(q, 16) * GROUPS + lax.div(lax.rem(q, 16), 2)).astype(F32)
@@ -326,11 +333,11 @@
     for copy in x_sends:
         copy.wait()
     stretch = [xarr[k] for k in range(nx)]
-    before = unit
-    total = stretch[0]
-    for k in range(1, nx):
-        before = jnp.where(x == k, total.astype(F32), before)
-        total = joined(stretch[k], total)
+    level = stretch
+    while len(level) > 1:
+        pairs = [joined(level[k + 1], level[k]) for k in range(0, len(level) - 1, 2)]
+        level = pairs + [v.astype(F32) for v in level[2 * len(pairs) :]]
+    total = level[0]
     zs[...] = total.astype(BF16)
     for d in range(1, nz):
         @pl.when(z + d < nz)
@@ -339,26 +346,38 @@
                 zs, zarr.at[z], zsend.at[d - 1], zrecv.at[z], {"ep": (z + d) * nx + x}
             ).start()
 
+    before, upto = unit, stretch[0].astype(F32)
+    for k in range(1, nx):
+        before = jnp.where(x == k, upto, before)
+        if k < nx - 1:
+            upto = joined(stretch[k], upto)
     zsc[...] = mm(beside_identity(before).T, z_all)
 
     order = FAR_FIRST + (0,)
-
-    def ring(step, way):
+    middle = aps.shape[2] // 2
+    halves = (slice(0, middle), slice(middle, 2 * middle))
+
+    def ring(step, way, part):
         k = 3 * way + step
         to = lax.rem(y + (GROUPS - 1 if way else 1), GROUPS)
         slot = order.index(4 + step if way else 3 - step)
-        return remote(aps.at[slot], ring_in.at[k], rsum_s.at[k], rsum_r.at[k], {"tp": 2 * to + c})
+        return remote(
+            aps.at[slot, :, halves[part]], ring_in.at[k, :, halves[part]],
+            rsum_s.at[part, k], rsum_r.at[part, k], {"tp": 2 * to + c},
+        )
 
     def ring_on(step):
-        for way in range(2):
-            if step < 3 + way:
-                ring(step - 1, way).wait_recv()
-                slot = order.index(4 + step if way else 3 - step)
-                arrived = ring_in[3 * way + step - 1].astype(F32)
-                aps[slot] = (aps[slot].astype(F32) + arrived).astype(BF16)
-                ring(step, way).start()
-
-    def project_heads():
+        for part in range(2):
+            for way in range(2):
+                if step < 3 + way:
+                    ring(step - 1, way, part).wait_recv()
+                    slot = order.index(4 + step if way else 3 - step)
+                    arrived = ring_in[3 * way + step - 1, :, halves[part]].astype(F32)
+                    kept = aps[slot, :, halves[part]].astype(F32)
+                    aps[slot, :, halves[part]] = (kept + arrived).astype(BF16)
+                    ring(step, way, part).start()
+
+    def heads():
         for k in range(nz - 1):
             @pl.when(k < z)
             def _():
@@ -379,6 +398,9 @@
         heads_out = heads_out.T.astype(BF16)
         own_rows = out_a.shape[0]
         ho[...] = heads_out.reshape(GROUPS, 2, own_rows, HC)
+
+    def project():
+        own_rows = out_a.shape[0]
         ready(19, 20)
 
         half = GROUPS // 2
@@ -402,12 +424,14 @@
             pair_mix[k].wait()
             aps[at] = (mixed[k].reshape(half, own_rows, -1) + apr[at].astype(F32)).astype(BF16)
             if k == 0:
-                ring(0, 0).start()
-                ring(0, 1).start()
+                for part in range(2):
+                    for way in range(2):
+                        ring(0, way, part).start()
 
     @pl.when(z < nz // 2)
     def _():
-        project_heads()
+        heads()
+        project()
 
     drain(darr.at[c, 0 : n_ep - 1], drecv)
     pair_rows = remote(darr.at[c], darr.at[c], pair_s.at[4], pair_r.at[4], {"tp": other})
@@ -424,6 +448,14 @@
         ep[k % 2, k // 2] = routed[:, k * cols : (k + 1) * cols]
     pair_routed = remote(ep.at[1 - c], epr, pair_s.at[1], pair_r.at[1], {"tp": other})
     pair_routed.start()
+
+    @pl.when(z < nz // 2)
+    def _():
+        ring_on(1)
+
+    @pl.when(z >= nz // 2)
+    def _():
+        heads()
 
     pair_routed.wait()
     both = ep[c].astype(F32) + epr[...].astype(F32)
@@ -449,15 +481,19 @@
 
     @pl.when(z >= nz // 2)
     def _():
-        project_heads()
-
-    ring_on(1)
+        project()
+
+    @pl.when(z >= nz // 2)
+    def _():
+        ring_on(1)
+
     ring_on(2)
     ring_on(3)
 
     ready(20, 21)
-    ring(2, 0).wait_recv()
-    ring(3, 1).wait_recv()
+    for part in range(2):
+        ring(2, 0, part).wait_recv()
+        ring(3, 1, part).wait_recv()
     mix = aps[GROUPS - 1].astype(F32) + ring_in[2].astype(F32) + ring_in[6].astype(F32)
     scale = lax.rsqrt(jnp.mean(mix * mix, axis=1, keepdims=True) + NORM_EPSILON)
     out_a[...] = (mix * scale * png[...]).astype(BF16)
@@ -477,7 +513,8 @@
             drain(zs, zsend.at[d - 1])
     for way in range(2):
         for step in range(3 + way):
-            ring(step, way).wait_send()
+            for part in range(2):
+                ring(step, way, part).wait_send()
     drain(dout.at[0 : n_ep - 1], dsend)
     drain(es.at[0 : n_ep * GROUPS - 1], rsend)
 
@@ -541,8 +578,8 @@
                 pltpu.SemaphoreType.REGULAR,
                 dma((GROUPS - 1,)),
                 dma((GROUPS - 1,)),
-                dma((7,)),
-                dma((7,)),
+                dma((2, 7)),
+                dma((2, 7)),
                 dma,
                 dma,
                 dma((max(nx - 1, 1),)),

time: 43.3 us -> 42.6 us (0.984)
  the two profiles are of different devices: /device:TPU:256 before, /device:TPU:1 now
where the time goes in v5:
time: 42.6 us; the launch traced here: 42.5 us
  Pallas kernels  40.6 us (95%)
  local copies, waits for them, and re-layouts  1.25 us (3%)
  between operations  0.65 us (2%)
    pallas_call x1, Pallas kernels, body(): pl.pallas_call(functools.partial(kernel, nx, nz), out_shape=(jax.ShapeDty...  40.6 us
    unnamed x2, local copies, waits for them, and re-layouts  1.25 us

profile of v5, /device:TPU:1, one launch (start us, length us, event | category | flops | bytes accessed | tf_op | source)
XLA Modules:
  0.0 42.5 jit_solution(17749576870390728478)
XLA Ops:
  0.6 40.6 %shard_map.212 = (bf16[16,2048]{1,0:T(8,128)(2,1)S(1)}, bf16[128,128]{1,0:T(8,128)(2,1)S(1)}) custom-call(bf16[128,2048]{1,0:T(8,128)(2,1)} %refs_0_.1, f32[1,2048]{1,0:T(1,128)} %bitcast.30, s32[2,128]{1,0:T(2,128)} %bitcast.32, bf16[64,2048]{1,0:T(8,128)(2,1)} %bitcast.21, bf16[64,2048]{1,0:T(8,128)(2,1)} %bitcast.22, bf16[64,2048]{1,0:T(8,128)(2,1)} %refs_5_.1, ...), custom_call_target="tpu_custom_call" | custom-call | tf_op jit(solution)/shard_map/pallas_call | solution.py:544
  41.2 0.6 %copy.25 = bf16[16,2048]{1,0:T(8,128)(2,1)} copy(bf16[16,2048]{1,0:T(8,128)(2,1)S(1)} %get-tuple-element.4) | data formatting | bytes 131072
  41.9 0.6 %copy.26 = bf16[128,128]{1,0:T(8,128)(2,1)} copy(bf16[128,128]{1,0:T(8,128)(2,1)S(1)} %get-tuple-element.5) | data formatting | bytes 65536
